TPU v7x, 32 devices: a whole 2x2x4 slice. The times are simulated.
32 devices in a mesh: sp: 8 (over z, core), tp: 4 (over y, x).
Axes of the slice: x: 2, y: 2, z: 4, core: 2. Of those that a mesh axis runs over, the one named last changes fastest.
Arguments:
- moe_in: bfloat16 [1536, 2048], P('sp'), may hold values from -6 to 6
- cotangent: bfloat16 [1536, 2048], P('sp'), may hold values from -6 to 6
- routing: int32 [1536, 2], P('sp'), may hold values from 0 to 7, as said below
- route_weight: float32 [1536, 2], P('sp'), may hold values from 0.2 to 1
- w_gate: bfloat16 [8, 2048, 2048], P('sp', 'tp'), may hold values from -0.125 to 0.125
- w_up: bfloat16 [8, 2048, 2048], P('sp', 'tp'), may hold values from -0.125 to 0.125
- w_down: bfloat16 [8, 2048, 2048], P('sp', 'tp'), may hold values from -0.125 to 0.125
- gate_b: bfloat16 [1024, 1536], P('tp', 'sp'), may hold values from -6 to 6
- gate_c: bfloat16 [1024, 1536], P('tp', 'sp'), may hold values from -6 to 6
- value_x: bfloat16 [1024, 1536], P('tp', 'sp'), may hold values from -6 to 6
- conv_taps: float32 [3, 1024], P(None, 'tp'), may hold values from -3 to 3
- out_proj: bfloat16 [1024, 2048], P('tp'), may hold values from -0.1875 to 0.1875
Outputs:
- w_gate_grad: bfloat16 [8, 2048, 2048], P('sp', 'tp')
- w_up_grad: bfloat16 [8, 2048, 2048], P('sp', 'tp')
- w_down_grad: bfloat16 [8, 2048, 2048], P('sp', 'tp')
- moe_in_grad: bfloat16 [1536, 2048], P('sp', 'tp')
- proj_grad: float32 [1024, 2048], P('tp', 'sp')
- gate_b_grad: bfloat16 [1024, 1536], P('tp', 'sp')
- gate_c_grad: bfloat16 [1024, 1536], P('tp', 'sp')
- value_x_grad: bfloat16 [1024, 1536], P('tp', 'sp')
Inputs may be any that keep to these rules, and one draw needn't show every extreme that they name: `routing`: in each aligned block of 192 rows every expert is named exactly 48 times. The two entries of a row are different experts of one group; group g holds experts g * 2 to g * 2 + 1.
All inputs are finite; a program needn't handle non-finite values.
Results may differ from a plain program's by a relative error of at most 0.025.
Values may be sent and summed in bfloat16 or wider, within the bound.
No kernel may reach another device: no remote copies, remote signals or barrier semaphores. Data moves between devices by JAX's collectives and lax.ppermute only.
A program may use at most 64 MiB of HBM per device.

v0:
```python
import jax
import jax.numpy as jnp
from jax import lax
from jax.sharding import PartitionSpec as P

TAPS = 3


def from_behind(array, axis, by):
    count = lax.axis_size(axis)
    pairs = [(i, i + by) for i in range(count) if 0 <= i + by < count]
    return lax.ppermute(array, axis, pairs)


def on_device(
    moe_in,
    cotangent,
    routing,
    route_weight,
    w_gate,
    w_up,
    w_down,
    gate_b,
    gate_c,
    value_x,
    conv_taps,
    out_proj,
):
    tok_rows = routing.shape[0]
    top_routes = routing.shape[1]
    experts = lax.axis_size("sp")
    lane_count = lax.axis_size("tp")
    model_width = moe_in.shape[1]
    capacity = top_routes * tok_rows // experts
    flat_routes = routing.reshape(-1)
    route_count = flat_routes.shape[0]
    one_hot = (flat_routes[:, None] == jnp.arange(experts, dtype=jnp.int32)[None, :]).astype(
        jnp.int32
    )
    slot_rank = jnp.sum(jnp.cumsum(one_hot, axis=0) * one_hot, axis=1) - 1
    slot_index = flat_routes * capacity + slot_rank
    source = (
        jnp.zeros((route_count,), jnp.int32)
        .at[slot_index]
        .set(jnp.arange(route_count, dtype=jnp.int32))
    )
    owner_token = source // top_routes
    scales = route_weight.reshape(-1)[source][:, None]
    col_width = model_width // lane_count
    col_start = lax.axis_index("tp") * col_width
    rows_part = lax.dynamic_slice_in_dim(moe_in, col_start, col_width, 1)[owner_token]
    cot_slice = lax.dynamic_slice_in_dim(cotangent, col_start, col_width, 1)[owner_token]
    cot_part = (scales * cot_slice.astype(jnp.float32)).astype(jnp.bfloat16)
    moved = (
        lax.all_to_all(rows_part, "sp", split_axis=0, concat_axis=0, tiled=True),
        lax.all_to_all(cot_part, "sp", split_axis=0, concat_axis=0, tiled=True),
    )
    arrived, arrived_cot = (
        lax.all_gather(moved[0], "tp", axis=1, tiled=True),
        lax.all_gather(moved[1], "tp", axis=1, tiled=True),
    )
    contract_model = (((1,), (1,)), ((), ()))
    over_rows = (((0,), (0,)), ((), ()))
    gate_pre = lax.dot_general(
        arrived, w_gate[0], contract_model, preferred_element_type=jnp.float32
    )
    up_pre = lax.dot_general(arrived, w_up[0], contract_model, preferred_element_type=jnp.float32)
    sigmoid_gate = jax.nn.sigmoid(gate_pre)
    hidden = (gate_pre * sigmoid_gate * up_pre).astype(jnp.bfloat16)
    hidden_grad = lax.dot_general(
        arrived_cot, w_down[0], contract_model, preferred_element_type=jnp.float32
    )
    gate_grad = (
        hidden_grad * up_pre * sigmoid_gate * (1.0 + gate_pre * (1.0 - sigmoid_gate))
    ).astype(jnp.bfloat16)
    up_grad = (hidden_grad * gate_pre * sigmoid_gate).astype(jnp.bfloat16)
    w_gate_grad = lax.dot_general(
        gate_grad, arrived, over_rows, preferred_element_type=jnp.float32
    ).astype(jnp.bfloat16)[None]
    w_up_grad = lax.dot_general(
        up_grad, arrived, over_rows, preferred_element_type=jnp.float32
    ).astype(jnp.bfloat16)[None]
    w_down_grad = lax.dot_general(
        hidden, arrived_cot, over_rows, preferred_element_type=jnp.float32
    ).astype(jnp.bfloat16)[None]
    partial_value = jnp.dot(gate_grad, w_gate[0], preferred_element_type=jnp.float32) + jnp.dot(
        up_grad, w_up[0], preferred_element_type=jnp.float32
    )
    partial_value = lax.optimization_barrier(partial_value.astype(jnp.bfloat16)).astype(jnp.float32)
    summed = lax.psum_scatter(
        partial_value.astype(jnp.bfloat16), "tp", scatter_dimension=1, tiled=True
    )
    returned = lax.all_to_all(summed, "sp", split_axis=0, concat_axis=0, tiled=True)
    per_route = returned[slot_index].astype(jnp.float32)
    moe_in_grad = jnp.sum(per_route.reshape(tok_rows, top_routes, -1), axis=1).astype(jnp.bfloat16)
    full_grad = lax.all_gather(moe_in_grad, "tp", axis=1, tiled=True)
    stream_grad = (cotangent.astype(jnp.float32) + full_grad.astype(jnp.float32)).astype(
        jnp.bfloat16
    )
    mixed_in = lax.optimization_barrier(
        (gate_c.astype(jnp.float32) * value_x.astype(jnp.float32)).astype(jnp.bfloat16)
    )
    earlier = from_behind(mixed_in[:, tok_rows - (TAPS - 1) :], "sp", 1)
    extended = jnp.concatenate([earlier, mixed_in], axis=1).astype(jnp.float32)
    conv_out = jnp.zeros(mixed_in.shape, jnp.float32)
    for tap in range(TAPS):
        conv_out = conv_out + conv_taps[tap][:, None] * extended[:, tap : tap + tok_rows]
    mixer_act = (gate_b.astype(jnp.float32) * conv_out).astype(jnp.bfloat16)
    act_grad = lax.dot_general(
        out_proj, stream_grad, contract_model, preferred_element_type=jnp.float32
    )
    proj_rows = lax.psum_scatter(
        lax.dot_general(
            stream_grad, mixer_act, (((0,), (1,)), ((), ())), preferred_element_type=jnp.float32
        ).astype(jnp.bfloat16),
        "sp",
        scatter_dimension=0,
        tiled=True,
    ).astype(jnp.float32)
    proj_grad = proj_rows.T
    gate_b_grad = (act_grad * conv_out).astype(jnp.bfloat16)
    conv_grad = act_grad * gate_b.astype(jnp.float32)
    later = from_behind(conv_grad[:, : TAPS - 1], "sp", -1)
    extended_grad = jnp.concatenate([conv_grad, later], axis=1)
    mixed_grad = jnp.zeros(conv_grad.shape, jnp.float32)
    for tap in range(TAPS):
        offset = TAPS - 1 - tap
        mixed_grad = (
            mixed_grad + conv_taps[tap][:, None] * extended_grad[:, offset : offset + tok_rows]
        )
    gate_c_grad = (mixed_grad * value_x.astype(jnp.float32)).astype(jnp.bfloat16)
    value_x_grad = (mixed_grad * gate_c.astype(jnp.float32)).astype(jnp.bfloat16)
    return (
        w_gate_grad,
        w_up_grad,
        w_down_grad,
        moe_in_grad,
        proj_grad,
        gate_b_grad,
        gate_c_grad,
        value_x_grad,
    )


def solution(mesh):
    in_specs = (
        P("sp", None),
        P("sp", None),
        P("sp", None),
        P("sp", None),
        P("sp", "tp", None),
        P("sp", "tp", None),
        P("sp", "tp", None),
        P("tp", "sp"),
        P("tp", "sp"),
        P("tp", "sp"),
        P(None, "tp"),
        P("tp", None),
    )
    out_specs = (
        P("sp", "tp", None),
        P("sp", "tp", None),
        P("sp", "tp", None),
        P("sp", "tp"),
        P("tp", "sp"),
        P("tp", "sp"),
        P("tp", "sp"),
        P("tp", "sp"),
    )
    return jax.shard_map(
        on_device, mesh=mesh, in_specs=in_specs, out_specs=out_specs, check_vma=False
    )
```

profile of v0, /device:TPU:0, one launch (start us, length us, event | category | flops | bytes accessed | tf_op | source)
XLA Modules:
  0.0 214.4 jit_solution(2672722682063082941)
XLA Ops:
  7.2 0.9 copy.23
  10.7 2.9 %scatter_custom_fusion = s32[384]{0:T(512)S(1)} fusion(s32[384]{0:T(512)S(1)} %fusion.30, s32[384]{0:T(512)S(1)} %iota.11, s32[]{:T(128)} %constant.15.clone.1), kind=kCustom, calls=%fused_computation.78 | custom fusion | bytes 1540 | tf_op jit(solution)/shard_map/scatter | solution.py:45
  13.6 1.1 constant_dynamic-slice_fusion
  14.7 2.1 gather_fusion.2
  16.8 18.8 %all_to_all.33 = bf16[8,48,512]{2,1,0:T(8,128)(2,1)} all-to-all(bf16[8,48,512]{2,1,0:T(8,128)(2,1)S(1)} %bitcast.57), channel_id=1, replica_groups=mesh['sp'=8,'tp'=4] {'sp'}, dimensions={0} | all-to-all | bytes 786432 | tf_op jit(solution)/shard_map/all_to_all | solution.py:55
  35.6 2.1 gather_fusion.1
  38.0 2.8 %gather_fusion = f32[384]{0:T(512)S(1)} fusion(f32[384]{0:T(512)S(1)} %reshape.90, s32[1024]{0:T(1024)S(1)} %get-tuple-element.39), kind=kCustom, calls=%fused_computation | custom fusion | bytes 4608 | tf_op jit(solution)/shard_map/gather | solution.py:48
  41.0 15.6 %all_to_all.34 = bf16[8,48,512]{2,1,0:T(8,128)(2,1)} all-to-all(bf16[8,48,512]{2,1,0:T(8,128)(2,1)S(1)} %fusion.12), channel_id=1, replica_groups=mesh['sp'=8,'tp'=4] {'sp'}, dimensions={0} | all-to-all | bytes 786432 | tf_op jit(solution)/shard_map/all_to_all | solution.py:56
  56.7 8.7 %all-gather.5.cloned.1.call-done = bf16[384,2048]{1,0:T(8,128)(2,1)} async-done(((bf16[384,512]{1,0:T(8,128)(2,1)}), bf16[384,2048]{1,0:T(8,128)(2,1)}) %all-gather.5.cloned.1.call-update) | async-done | bytes 1572880 | tf_op jit(solution)/shard_map/all_gather | solution.py:59
  65.4 2.6 %fusion.5 = f32[384,512]{1,0:T(8,128)S(1)} fusion(bf16[384,2048]{1,0:T(8,128)(2,1)} %all-gather.5.cloned.1.call-done, bf16[1,512,2048]{2,1,0:T(8,128)(2,1)S(1)} %copy-done), kind=kOutput, calls=%fused_computation.15 | convolution fusion | flops 805306368 | bytes 4456448 | tf_op jit(solution)/shard_map/dot_general | solution.py:64
  68.0 1.9 fusion.8
  69.9 28.1 %all-gather.3.cloned.1.call-done = bf16[384,2048]{1,0:T(8,128)(2,1)} async-done(((bf16[384,512]{1,0:T(8,128)(2,1)}), bf16[384,2048]{1,0:T(8,128)(2,1)}) %all-gather.3.cloned.1.call-update) | async-done | bytes 1572880 | tf_op jit(solution)/shard_map/all_gather | solution.py:60
  97.9 3.4 %multiply_convert_fusion.1 = (bf16[384,512]{1,0:T(8,128)(2,1)S(1)}, bf16[384,512]{1,0:T(8,128)(2,1)S(1)}) fusion(f32[384,512]{1,0:T(8,128)S(1)} %fusion.5, f32[384,512]{1,0:T(8,128)} %fusion.8, bf16[384,2048]{1,0:T(8,128)(2,1)} %all-gather.3.cloned.1.call-done, bf16[1,512,2048]{2,1,0:T(8,128)(2,1)} %param.18), kind=kOutput, calls=%fused_computation.27 | convolution fusion | flops 807862272 | bytes 6029312 | tf_op jit(solution)/shard_map/dot_general | solution.py:70
  101.4 1.0 fusion.3
  102.4 0.9 copy-done.3
  103.3 2.1 add_convert_fusion
  105.4 31.3 %reduce-scatter.3.cloned.1.call-done = bf16[384,512]{1,0:T(8,128)(2,1)} async-done(((bf16[384,2048]{1,0:T(8,128)(2,1)}), bf16[384,512]{1,0:T(8,128)(2,1)}) %reduce-scatter.3.cloned.1.call-update) | async-done | bytes 393232 | tf_op jit(solution)/shard_map/reduce_scatter | solution.py:90
  136.7 4.6 %all-to-all-start.2 = ((bf16[8,48,512]{2,1,0:T(8,128)(2,1)}), bf16[8,48,512]{2,1,0:T(8,128)(2,1)S(1)}, u32[]{:S(2)}, u32[]{:S(2)}) async-start(bf16[8,48,512]{2,1,0:T(8,128)(2,1)} %bitcast.58), calls=%async_computation.3 | async-start | bytes 786432 | tf_op jit(solution)/shard_map/all_to_all | solution.py:93
  141.4 2.4 %collective-permute-start = (bf16[256,2]{0,1:T(2,128)(2,1)S(1)}, bf16[256,2]{0,1:T(2,128)(2,1)S(1)}, u32[]{:S(2)}, u32[]{:S(2)}) collective-permute-start(bf16[256,2]{0,1:T(2,128)(2,1)S(1)} %slice.60), channel_id=1, source_target_pairs={{0,4},{4,8},{8,12},{12,16},{16,20},{20,24},{24,28},{1,5},{5,9},{9,... | collective-permute-start | bytes 3080 | tf_op jit(solution)/shard_map/ppermute | solution.py:12
  144.6 9.2 %all-to-all-done.2 = bf16[8,48,512]{2,1,0:T(8,128)(2,1)S(1)} async-done(((bf16[8,48,512]{2,1,0:T(8,128)(2,1)}), bf16[8,48,512]{2,1,0:T(8,128)(2,1)S(1)}, u32[]{:S(2)}, u32[]{:S(2)}) %all-to-all-start.2) | async-done | bytes 393248 | tf_op jit(solution)/shard_map/all_to_all | solution.py:93
  153.8 2.6 %gather_fusion.3 = bf16[384,512]{1,0:T(8,128)(2,1)} fusion(bf16[384,512]{1,0:T(8,128)(2,1)S(1)} %bitcast.53, s32[1024]{0:T(1024)S(1)} %pad_clamp_fusion), kind=kCustom, calls=%fused_computation.3 | custom fusion | bytes 787968 | tf_op jit(solution)/shard_map/gather | solution.py:94
  156.4 1.1 gather.18
  157.6 1.7 reduce_sum.22
  159.3 11.3 %all_gather.11 = bf16[192,2048]{1,0:T(8,128)(2,1)S(1)} all-gather(bf16[192,512]{1,0:T(8,128)(2,1)} %reduce_sum.22), channel_id=1, replica_groups=mesh['sp'=8,'tp'=4] {'tp'}, dimensions={1}, use_global_device_ids=true | all-gather | bytes 983040 | tf_op jit(solution)/shard_map/all_gather | solution.py:96
  170.6 2.4 %multiply_convert_fusion.4 = (bf16[256,192]{0,1:T(8,128)(2,1)}, f32[256,192]{0,1:T(8,128)S(1)}, f32[256,192]{0,1:T(8,128)S(1)}) fusion(f32[256,194]{0,1:T(8,128)S(1)} %maximum_convert_fusion, f32[256]{0:T(256)S(1)} %bitcast.61, f32[256]{0:T(256)S(1)} %bitcast.63, f32[256]{0:T(256)S(1)} %bitcast.59, bf16[256,192]{0,1:T(8,128)(2,1)} %param.19, ...), kind=kOutput, calls=%fused_computation.54 | convolution fusion | flops 203341824 | bytes 3804160 | tf_op jit(solution)/shard_map/dot_general | solution.py:109
  173.0 1.5 convolution_convert_fusion.3
  174.6 4.3 %fusion.1 = bf16[1,512,2048]{2,1,0:T(8,128)(2,1)} fusion(bf16[384,512]{1,0:T(8,128)(2,1)} %copy-done.4, bf16[384,2048]{1,0:T(8,128)(2,1)} %all-gather.5.cloned.1.call-done), kind=kOutput, calls=%fused_computation.10 | convolution fusion | flops 806354944 | bytes 4063232 | tf_op jit(solution)/shard_map/dot_general | solution.py:80
  178.9 2.7 %fusion.2 = bf16[1,512,2048]{2,1,0:T(8,128)(2,1)} fusion(bf16[384,2048]{1,0:T(8,128)(2,1)S(1)} %copy-done.16, f32[384,512]{1,0:T(8,128)S(1)} %copy-done.19, f32[384,512]{1,0:T(8,128)S(1)} %copy-done.18), kind=kOutput, calls=%fused_computation.11 | convolution fusion | flops 807534592 | bytes 5242880 | tf_op jit(solution)/shard_map/dot_general | solution.py:83
  181.6 1.4 collective-permute-start.1
  183.0 2.6 %fusion = bf16[1,512,2048]{2,1,0:T(8,128)(2,1)} fusion(bf16[384,512]{1,0:T(8,128)(2,1)S(1)} %copy-done.11, bf16[384,2048]{1,0:T(8,128)(2,1)S(1)} %copy-done.15), kind=kOutput, calls=%fused_computation.9 | convolution fusion | flops 806354944 | bytes 4063232 | tf_op jit(solution)/shard_map/dot_general | solution.py:77
  187.0 19.0 %reduce-scatter.5.cloned.1.call-done = bf16[256,256]{1,0:T(8,128)(2,1)} async-done(((bf16[2048,256]{1,0:T(8,128)(2,1)}), bf16[256,256]{1,0:T(8,128)(2,1)}) %reduce-scatter.5.cloned.1.call-update) | async-done | bytes 131088 | tf_op jit(solution)/shard_map/reduce_scatter | solution.py:112
  206.1 0.9 convert_bitcast_fusion
  (77 shorter events, 6.4 us)
Async XLA Ops:
  7.2 58.2 %copy-start = (bf16[1,512,2048]{2,1,0:T(8,128)(2,1)S(1)}, bf16[1,512,2048]{2,1,0:T(8,128)(2,1)}, u32[]{:S(2)}) copy-start(bf16[1,512,2048]{2,1,0:T(8,128)(2,1)} %param.16) | copy-start | bytes 6291460
  7.2 58.2 %all-gather.5.cloned.1.call-start = ((), (), s32[]{:S(2)}) async-start(), calls=%async_computation.6 | async-start | bytes 1966080 | tf_op jit(solution)/shard_map/all_gather | solution.py:59
  35.5 2.2 %copy-start.13 = (f32[192,2]{0,1:T(2,128)S(1)}, f32[192,2]{0,1:T(2,128)}, u32[]{:S(2)}) copy-start(f32[192,2]{0,1:T(2,128)} %param.15) | copy-start | bytes 4612
  35.6 62.4 %all-gather.3.cloned.1.call-start = ((), (), s32[]{:S(2)}) async-start(), calls=%async_computation.5 | async-start | bytes 1966080 | tf_op jit(solution)/shard_map/all_gather | solution.py:60
  56.6 80.1 %reduce-scatter.3.cloned.1.call-start = ((), (), s32[]{:S(2)}) async-start(), calls=%async_computation.7 | async-start | bytes 1966080 | tf_op jit(solution)/shard_map/reduce_scatter | solution.py:90
  65.4 2.6 %copy-start.2 = (bf16[1,512,2048]{2,1,0:T(8,128)(2,1)S(1)}, bf16[1,512,2048]{2,1,0:T(8,128)(2,1)}, u32[]{:S(2)}) copy-start(bf16[1,512,2048]{2,1,0:T(8,128)(2,1)} %param.17) | copy-start | bytes 6291460
  65.4 2.6 %copy-start.14 = (bf16[384,2048]{1,0:T(8,128)(2,1)S(1)}, bf16[384,2048]{1,0:T(8,128)(2,1)}, u32[]{:S(2)}) copy-start(bf16[384,2048]{1,0:T(8,128)(2,1)} %all-gather.5.cloned.1.call-done) | copy-start | bytes 4718596
  68.0 30.0 %copy-start.17 = (f32[384,512]{1,0:T(8,128)}, f32[384,512]{1,0:T(8,128)S(1)}, u32[]{:S(2)}) copy-start(f32[384,512]{1,0:T(8,128)S(1)} %fusion.5) | copy-start | bytes 2359300
  101.4 1.0 copy-start.10
  101.4 1.0 copy-start.4
  101.4 1.9 copy-start.3
  105.4 36.0 %copy-start.6 = (bf16[256,192]{0,1:T(8,128)(2,1)S(1)}, bf16[256,192]{0,1:T(8,128)(2,1)}, u32[]{:S(2)}) copy-start(bf16[256,192]{0,1:T(8,128)(2,1)} %param.20) | copy-start | bytes 294916
  105.4 36.0 %copy-start.8 = (bf16[256,192]{0,1:T(8,128)(2,1)S(1)}, bf16[256,192]{0,1:T(8,128)(2,1)}, u32[]{:S(2)}) copy-start(bf16[256,192]{0,1:T(8,128)(2,1)} %param.21) | copy-start | bytes 294916
  105.4 38.4 %copy-start.12 = (f32[3,256]{1,0:T(4,128)S(1)}, f32[3,256]{1,0:T(4,128)}, u32[]{:S(2)}) copy-start(f32[3,256]{1,0:T(4,128)} %param.22) | copy-start | bytes 9220
  136.7 17.1 %all-to-all-start.2 = ((bf16[8,48,512]{2,1,0:T(8,128)(2,1)}), bf16[8,48,512]{2,1,0:T(8,128)(2,1)S(1)}, u32[]{:S(2)}, u32[]{:S(2)}) async-start(bf16[8,48,512]{2,1,0:T(8,128)(2,1)} %bitcast.58), calls=%async_computation.3 | async-start | bytes 786432 | tf_op jit(solution)/shard_map/all_to_all | solution.py:93
  141.3 64.8 %reduce-scatter.5.cloned.1.call-start = ((), (), s32[]{:S(2)}) async-start(), calls=%async_computation.8 | async-start | bytes 1179648 | tf_op jit(solution)/shard_map/reduce_scatter | solution.py:112
  141.4 3.2 %collective-permute-start = (bf16[256,2]{0,1:T(2,128)(2,1)S(1)}, bf16[256,2]{0,1:T(2,128)(2,1)S(1)}, u32[]{:S(2)}, u32[]{:S(2)}) collective-permute-start(bf16[256,2]{0,1:T(2,128)(2,1)S(1)} %slice.60), channel_id=1, source_target_pairs={{0,4},{4,8},{8,12},{12,16},{16,20},{20,24},{24,28},{1,5},{5,9},{9,... | collective-permute-start | bytes 3080 | tf_op jit(solution)/shard_map/ppermute | solution.py:12
  153.8 16.8 %copy-start.1 = (bf16[192,2048]{1,0:T(8,128)(2,1)S(1)}, bf16[192,2048]{1,0:T(8,128)(2,1)}, u32[]{:S(2)}) copy-start(bf16[192,2048]{1,0:T(8,128)(2,1)} %param.13) | copy-start | bytes 2359300
  159.3 13.7 %copy-start.5 = (bf16[256,192]{0,1:T(8,128)(2,1)S(1)}, bf16[256,192]{0,1:T(8,128)(2,1)}, u32[]{:S(2)}) copy-start(bf16[256,192]{0,1:T(8,128)(2,1)} %param.19) | copy-start | bytes 294916
  174.6 4.3 %copy-start.16 = (bf16[384,2048]{1,0:T(8,128)(2,1)S(1)}, bf16[384,2048]{1,0:T(8,128)(2,1)}, u32[]{:S(2)}) copy-start(bf16[384,2048]{1,0:T(8,128)(2,1)} %all-gather.3.cloned.1.call-done) | copy-start | bytes 4718596
  174.6 4.3 %copy-start.18 = (f32[384,512]{1,0:T(8,128)S(1)}, f32[384,512]{1,0:T(8,128)}, u32[]{:S(2)}) copy-start(f32[384,512]{1,0:T(8,128)} %copy-done.17) | copy-start | bytes 2359300
  174.6 4.3 %copy-start.19 = (f32[384,512]{1,0:T(8,128)S(1)}, f32[384,512]{1,0:T(8,128)}, u32[]{:S(2)}) copy-start(f32[384,512]{1,0:T(8,128)} %fusion.8) | copy-start | bytes 2359300
  178.9 4.1 %copy-start.11 = (bf16[384,512]{1,0:T(8,128)(2,1)S(1)}, bf16[384,512]{1,0:T(8,128)(2,1)}, u32[]{:S(2)}) copy-start(bf16[384,512]{1,0:T(8,128)(2,1)} %copy-done.10) | copy-start | bytes 1179652
  178.9 4.1 %copy-start.15 = (bf16[384,2048]{1,0:T(8,128)(2,1)S(1)}, bf16[384,2048]{1,0:T(8,128)(2,1)}, u32[]{:S(2)}) copy-start(bf16[384,2048]{1,0:T(8,128)(2,1)} %all-gather.5.cloned.1.call-done) | copy-start | bytes 4718596
  181.6 4.1 %copy-start.7 = (bf16[256,192]{0,1:T(8,128)(2,1)S(1)}, bf16[256,192]{0,1:T(8,128)(2,1)}, u32[]{:S(2)}) copy-start(bf16[256,192]{0,1:T(8,128)(2,1)} %param.20) | copy-start | bytes 294916
  181.6 4.8 %copy-start.9 = (bf16[256,192]{0,1:T(8,128)(2,1)S(1)}, bf16[256,192]{0,1:T(8,128)(2,1)}, u32[]{:S(2)}) copy-start(bf16[256,192]{0,1:T(8,128)(2,1)} %param.21) | copy-start | bytes 294916
  181.6 4.1 %collective-permute-start.1 = (f32[256,2]{0,1:T(2,128)S(1)}, f32[256,2]{0,1:T(2,128)S(1)}, u32[]{:S(2)}, u32[]{:S(2)}) collective-permute-start(f32[256,2]{0,1:T(2,128)S(1)} %slice.64), channel_id=1, source_target_pairs={{4,0},{8,4},{12,8},{16,12},{20,16},{24,20},{28,24},{5,1},{9,5},{13... | collective-permute-start | bytes 6152 | tf_op jit(solution)/shard_map/ppermute | solution.py:12
Sparse Core Ops, SparseCore 0:
  35.7 29.6 all-gather.4
  67.2 30.6 all-gather.2
  105.5 31.1 reduce-scatter.2
  174.7 31.3 reduce-scatter.4
where the time goes:
time: 215 us; the launch traced here: 214 us
  waiting for transfers between devices  97.1 us (45%)
  blocking collectives  45.7 us (21%)
  matrix products  24.5 us (11%)
  local copies, waits for them, and re-layouts  18.5 us (9%)
  between operations  14.1 us (7%)
  starting transfers between devices  8.54 us (4%)
  other arithmetic  5.94 us (3%)
    reduce_scatter x1, waiting for transfers between devices, on_device(): lax.psum_scatter(partial_value.astype(jnp.bfloat16), 'tp', scatter_dimens...  31.3 us
    all_gather x1, waiting for transfers between devices, on_device(): lax.all_gather(moved[1], 'tp', axis=1, tiled=True)  28.1 us
    reduce_scatter x1, waiting for transfers between devices, on_device(): lax.psum_scatter(lax.dot_general(stream_grad, mixer_act, (((0,), (1,)), (...  19 us
    all_to_all x1, blocking collectives, on_device(): lax.all_to_all(rows_part, 'sp', split_axis=0, concat_axis=0, tiled=True)  18.8 us
    all_to_all x1, blocking collectives, on_device(): lax.all_to_all(cot_part, 'sp', split_axis=0, concat_axis=0, tiled=True)  15.6 us
    all_gather x1, blocking collectives, on_device(): full_grad = lax.all_gather(moe_in_grad, 'tp', axis=1, tiled=True)  11.3 us
    all_to_all x1, waiting for transfers between devices, on_device(): lax.all_to_all(summed, 'sp', split_axis=0, concat_axis=0, tiled=True)  9.21 us
    all_gather x1, waiting for transfers between devices, on_device(): lax.all_gather(moved[0], 'tp', axis=1, tiled=True)  8.69 us
  transfers between devices with their start and end apart: 7, of which 6 were waited for; matrix products, arithmetic and copies ran while one was open for 10% of the time, Pallas kernels for 0%

commit v1 on v0

v1 whole, which is shorter than its diff:
```python
import jax
import jax.numpy as jnp
from jax import lax
from jax.sharding import Mesh
from jax.sharding import PartitionSpec as P

TAPS = 3
GROUPS = 4
CORES = 2
BF = jnp.bfloat16
F32 = jnp.float32
SP = ("z", "c")


def from_behind(array, by):
    count = lax.axis_size(SP)
    pairs = [(i, i + by) for i in range(count) if 0 <= i + by < count]
    return lax.ppermute(array, SP, pairs)


def partner(array, axis, bit):
    count = lax.axis_size(axis)
    return lax.ppermute(array, axis, [(i, i ^ bit) for i in range(count)])


def dot(a, b, ca, cb, kind=F32):
    return lax.dot_general(a, b, (((ca,), (cb,)), ((), ())), preferred_element_type=F32).astype(kind)


def shared_plan(sp, tp, top_routes):
    return top_routes == CORES and GROUPS * CORES == sp and tp == GROUPS and tp & (tp - 1) == 0


def shared_rows(
    moe_in, cotangent, routing, route_weight, w_gate, w_up, w_down,
    gate_b, gate_c, value_x, conv_taps, out_proj,
):
    planes = lax.axis_size("z")
    lanes = lax.axis_size("tp")
    z, c, l = lax.axis_index("z"), lax.axis_index("c"), lax.axis_index("tp")
    rows, width = moe_in.shape
    cap = rows // planes
    cols = width // lanes
    half = cols // CORES
    at = l * cols

    group = routing[:, 0] // CORES
    hot = (group[:, None] == jnp.arange(planes)[None, :]).astype(BF)
    t = jnp.arange(rows)
    before = (t[:, None] > t[None, :]).astype(BF)
    rank = jnp.sum(dot(before, hot, 1, 0) * hot.astype(F32), axis=1).astype(jnp.int32)
    place = group * cap + rank
    perm = (place[:, None] == t[None, :]).astype(BF)

    core = routing % CORES
    weights = [jnp.sum(jnp.where(core == k, route_weight, 0.0), axis=1) for k in range(CORES)]
    weights = jnp.stack(weights, axis=1)
    high = weights.astype(BF)
    low = (weights - high.astype(F32)).astype(BF)
    parts = dot(jnp.concatenate([high, low], axis=1), perm, 0, 0, BF)
    parts = parts.reshape(2 * CORES, planes, cap).transpose(1, 0, 2).reshape(planes, 1, 2 * CORES * cap)
    parts = jnp.pad(parts, ((0, 0), (0, 15), (0, cols - 2 * CORES * cap)))

    x_rows = dot(perm, lax.dynamic_slice_in_dim(moe_in, at, cols, 1), 0, 0, BF)
    c_rows = dot(perm, lax.dynamic_slice_in_dim(cotangent, at, cols, 1), 0, 0, BF)
    sent = jnp.concatenate(
        [x_rows.reshape(planes, cap, cols), c_rows.reshape(planes, cap, cols), parts], axis=1
    )

    def over_planes(blocks):
        own = lax.dynamic_index_in_dim(blocks, z, 0, False)
        return [own] + [
            partner(lax.dynamic_index_in_dim(blocks, z ^ bit, 0, False), "z", bit)
            for bit in range(1, planes)
        ]

    got = over_planes(sent)
    x_own = jnp.concatenate([g[:cap] for g in got], axis=0)
    c_own = jnp.concatenate([g[cap : 2 * cap] for g in got], axis=0)
    w_own = jnp.concatenate(
        [g[2 * cap, : 2 * CORES * cap].reshape(2, CORES, cap) for g in got], axis=2
    ).astype(F32)
    w_own = w_own[0] + w_own[1]
    w_mine = lax.dynamic_index_in_dim(w_own, c, 0, False)
    w_other = lax.dynamic_index_in_dim(w_own, 1 - c, 0, False)
    w_far = partner(w_other, "c", 1)
    scale = jnp.concatenate([w_mine, w_far])[:, None]

    def over_lanes(piece):
        a, b = partner(piece, "tp", 1), partner(piece, "tp", 2)
        m = piece.shape[0] // 2
        d = jnp.concatenate([partner(b[:m], "tp", 1), partner(a[m:], "tp", 2)], axis=0)
        return [piece, a, b, d]

    def join(pieces):
        out = jnp.zeros((pieces[0].shape[0], width), pieces[0].dtype)
        for bit, piece in enumerate(pieces):
            out = lax.dynamic_update_slice_in_dim(out, piece, (l ^ bit) * cols, 1)
        return out

    x_near = join(over_lanes(x_own))
    c_near = join(over_lanes(c_own))
    arrived = jnp.concatenate([x_near, partner(x_near, "c", 1)], axis=0)
    arrived_cot = jnp.concatenate([c_near, partner(c_near, "c", 1)], axis=0)

    gate_pre = dot(arrived, w_gate[0], 1, 1)
    up_pre = dot(arrived, w_up[0], 1, 1)
    sig = jax.nn.sigmoid(gate_pre)
    hidden = gate_pre * sig * up_pre
    hidden_grad = scale * dot(arrived_cot, w_down[0], 1, 1)
    gate_grad = (hidden_grad * up_pre * sig * (1.0 + gate_pre * (1.0 - sig))).astype(BF)
    up_grad = (hidden_grad * gate_pre * sig).astype(BF)
    scaled_hidden = (scale * hidden).astype(BF)
    partial = dot(gate_grad, w_gate[0], 1, 0) + dot(up_grad, w_up[0], 1, 0)
    w_gate_grad = dot(gate_grad, arrived, 0, 0, BF)[None]
    w_up_grad = dot(up_grad, arrived, 0, 0, BF)[None]
    w_down_grad = dot(scaled_hidden, arrived_cot, 0, 0, BF)[None]

    partial = partial.astype(BF)
    near = partial[:rows].astype(F32) + partner(partial[rows:], "c", 1).astype(F32)
    near = near.astype(BF)
    total = lax.dynamic_slice_in_dim(near, at, cols, 1).astype(F32)
    for bit in range(1, lanes):
        piece = lax.dynamic_slice_in_dim(near, (l ^ bit) * cols, cols, 1)
        total = total + partner(piece, "tp", bit).astype(F32)
    total = total.astype(BF).reshape(planes, cap, cols)
    back = [total[0]] + [partner(total[bit], "z", bit) for bit in range(1, planes)]
    placed = jnp.stack(back)
    order = z ^ jnp.arange(planes)
    sorted_grad = jnp.zeros((planes, cap, cols), BF)
    for bit in range(planes):
        sorted_grad = lax.dynamic_update_index_in_dim(sorted_grad, back[bit], z ^ bit, 0)
    moe_in_grad = dot(perm, sorted_grad.reshape(rows, cols), 1, 0, BF)

    mixed_in = (gate_c.astype(F32) * value_x.astype(F32)).astype(BF)
    earlier = from_behind(mixed_in[:, rows - (TAPS - 1) :], 1)
    extended = jnp.concatenate([earlier, mixed_in], axis=1).astype(F32)
    conv_out = jnp.zeros(mixed_in.shape, F32)
    for tap in range(TAPS):
        conv_out = conv_out + conv_taps[tap][:, None] * extended[:, tap : tap + rows]
    mixer_act = (gate_b.astype(F32) * conv_out).astype(BF)
    acts = jnp.stack([mixer_act] + [partner(mixer_act, "tp", bit) for bit in range(1, lanes)])

    cot_part = lax.dynamic_slice_in_dim(cotangent, at, cols, 1)
    stream_part = (cot_part.astype(F32) + moe_in_grad.astype(F32)).astype(BF)
    share = dot(acts.reshape(-1, rows), stream_part, 1, 0).reshape(lanes, -1, cols)
    share_far = lax.dynamic_slice_in_dim(share, (1 - c) * half, half, 2).astype(BF)
    share_near = lax.dynamic_slice_in_dim(share, c * half, half, 2)
    share = (share_near + partner(share_far, "c", 1).astype(F32)).astype(BF)
    proj_grad = jnp.zeros(share.shape[1:], F32)
    for turn in range(lanes):
        piece = lax.dynamic_index_in_dim(share, l ^ z ^ turn, 0, False)
        pairs = [
            (a * lanes + b, b * lanes + (a ^ turn)) for a in range(planes) for b in range(lanes)
        ]
        proj_grad = proj_grad + lax.ppermute(piece, ("z", "tp"), pairs).astype(F32)

    full_grad = join([moe_in_grad] + [partner(moe_in_grad, "tp", bit) for bit in range(1, lanes)])
    stream_grad = (cotangent.astype(F32) + full_grad.astype(F32)).astype(BF)
    act_grad = dot(out_proj, stream_grad, 1, 1)
    gate_b_grad = (act_grad * conv_out).astype(BF)
    conv_grad = act_grad * gate_b.astype(F32)
    later = from_behind(conv_grad[:, : TAPS - 1], -1)
    extended_grad = jnp.concatenate([conv_grad, later], axis=1)
    mixed_grad = jnp.zeros(conv_grad.shape, F32)
    for tap in range(TAPS):
        offset = TAPS - 1 - tap
        mixed_grad = mixed_grad + conv_taps[tap][:, None] * extended_grad[:, offset : offset + rows]
    gate_c_grad = (mixed_grad * value_x.astype(F32)).astype(BF)
    value_x_grad = (mixed_grad * gate_c.astype(F32)).astype(BF)
    return (
        w_gate_grad, w_up_grad, w_down_grad, moe_in_grad, proj_grad,
        gate_b_grad, gate_c_grad, value_x_grad,
    )


def any_rows(
    moe_in, cotangent, routing, route_weight, w_gate, w_up, w_down,
    gate_b, gate_c, value_x, conv_taps, out_proj,
):
    tok_rows, top_routes = routing.shape
    experts = lax.axis_size(SP)
    lane_count = lax.axis_size("tp")
    model_width = moe_in.shape[1]
    capacity = top_routes * tok_rows // experts
    flat_routes = routing.reshape(-1)
    route_count = flat_routes.shape[0]
    one_hot = (flat_routes[:, None] == jnp.arange(experts, dtype=jnp.int32)[None, :]).astype(
        jnp.int32
    )
    slot_rank = jnp.sum(jnp.cumsum(one_hot, axis=0) * one_hot, axis=1) - 1
    slot_index = flat_routes * capacity + slot_rank
    source = (
        jnp.zeros((route_count,), jnp.int32)
        .at[slot_index]
        .set(jnp.arange(route_count, dtype=jnp.int32))
    )
    owner_token = source // top_routes
    scales = route_weight.reshape(-1)[source][:, None]
    col_width = model_width // lane_count
    col_start = lax.axis_index("tp") * col_width
    rows_part = lax.dynamic_slice_in_dim(moe_in, col_start, col_width, 1)[owner_token]
    cot_slice = lax.dynamic_slice_in_dim(cotangent, col_start, col_width, 1)[owner_token]
    cot_part = (scales * cot_slice.astype(F32)).astype(BF)
    moved = (
        lax.all_to_all(rows_part, SP, split_axis=0, concat_axis=0, tiled=True),
        lax.all_to_all(cot_part, SP, split_axis=0, concat_axis=0, tiled=True),
    )
    arrived, arrived_cot = (
        lax.all_gather(moved[0], "tp", axis=1, tiled=True),
        lax.all_gather(moved[1], "tp", axis=1, tiled=True),
    )
    gate_pre = dot(arrived, w_gate[0], 1, 1)
    up_pre = dot(arrived, w_up[0], 1, 1)
    sigmoid_gate = jax.nn.sigmoid(gate_pre)
    hidden = (gate_pre * sigmoid_gate * up_pre).astype(BF)
    hidden_grad = dot(arrived_cot, w_down[0], 1, 1)
    gate_grad = (
        hidden_grad * up_pre * sigmoid_gate * (1.0 + gate_pre * (1.0 - sigmoid_gate))
    ).astype(BF)
    up_grad = (hidden_grad * gate_pre * sigmoid_gate).astype(BF)
    w_gate_grad = dot(gate_grad, arrived, 0, 0, BF)[None]
    w_up_grad = dot(up_grad, arrived, 0, 0, BF)[None]
    w_down_grad = dot(hidden, arrived_cot, 0, 0, BF)[None]
    partial_value = dot(gate_grad, w_gate[0], 1, 0) + dot(up_grad, w_up[0], 1, 0)
    summed = lax.psum_scatter(partial_value.astype(BF), "tp", scatter_dimension=1, tiled=True)
    returned = lax.all_to_all(summed, SP, split_axis=0, concat_axis=0, tiled=True)
    per_route = returned[slot_index].astype(F32)
    moe_in_grad = jnp.sum(per_route.reshape(tok_rows, top_routes, -1), axis=1).astype(BF)
    full_grad = lax.all_gather(moe_in_grad, "tp", axis=1, tiled=True)
    stream_grad = (cotangent.astype(F32) + full_grad.astype(F32)).astype(BF)
    mixed_in = (gate_c.astype(F32) * value_x.astype(F32)).astype(BF)
    earlier = from_behind(mixed_in[:, tok_rows - (TAPS - 1) :], 1)
    extended = jnp.concatenate([earlier, mixed_in], axis=1).astype(F32)
    conv_out = jnp.zeros(mixed_in.shape, F32)
    for tap in range(TAPS):
        conv_out = conv_out + conv_taps[tap][:, None] * extended[:, tap : tap + tok_rows]
    mixer_act = (gate_b.astype(F32) * conv_out).astype(BF)
    act_grad = dot(out_proj, stream_grad, 1, 1)
    proj_rows = lax.psum_scatter(
        dot(stream_grad, mixer_act, 0, 1, BF), SP, scatter_dimension=0, tiled=True
    ).astype(F32)
    proj_grad = proj_rows.T
    gate_b_grad = (act_grad * conv_out).astype(BF)
    conv_grad = act_grad * gate_b.astype(F32)
    later = from_behind(conv_grad[:, : TAPS - 1], -1)
    extended_grad = jnp.concatenate([conv_grad, later], axis=1)
    mixed_grad = jnp.zeros(conv_grad.shape, F32)
    for tap in range(TAPS):
        offset = TAPS - 1 - tap
        mixed_grad = (
            mixed_grad + conv_taps[tap][:, None] * extended_grad[:, offset : offset + tok_rows]
        )
    gate_c_grad = (mixed_grad * value_x.astype(F32)).astype(BF)
    value_x_grad = (mixed_grad * gate_c.astype(F32)).astype(BF)
    return (
        w_gate_grad, w_up_grad, w_down_grad, moe_in_grad, proj_grad,
        gate_b_grad, gate_c_grad, value_x_grad,
    )


def solution(mesh):
    sp, tp = mesh.shape["sp"], mesh.shape["tp"]
    split = Mesh(mesh.devices.reshape(sp // CORES, CORES, tp), ("z", "c", "tp"))
    experts = P(SP, "tp", None)
    tokens = P(SP, None)
    mixer = P("tp", SP)

    def step(moe_in, cotangent, routing, *rest):
        body = shared_rows if shared_plan(sp, tp, routing.shape[1]) else any_rows
        return jax.shard_map(
            body,
            mesh=split,
            in_specs=(tokens,) * 4 + (experts,) * 3 + (mixer,) * 3 + (P(None, "tp"), P("tp", None)),
            out_specs=(experts,) * 3 + (P(SP, "tp"),) + (mixer,) * 4,
            check_vma=False,
        )(moe_in, cotangent, routing, *rest)

    return step
```

time: 215 us -> 156 us (0.73)
  the two profiles are of different devices: /device:TPU:0 before, /device:TPU:5 now
where the time goes in v1:
time: 156 us; the launch traced here: 155 us
  waiting for transfers between devices  58.8 us (38%)
  starting transfers between devices  51.5 us (33%)
  matrix products  25.6 us (16%)
  local copies, waits for them, and re-layouts  9.2 us (6%)
  other arithmetic  8.45 us (5%)
    ppermute x28, starting transfers between devices, partner(): return lax.ppermute(array, axis, [(i, i ^ bit) for i in range(count)])  35.3 us
    ppermute x4, waiting for transfers between devices, shared_rows(): proj_grad = proj_grad + lax.ppermute(piece, ('z', 'tp'), pairs).astype(F32)  30.2 us
    ppermute x28, waiting for transfers between devices, partner(): return lax.ppermute(array, axis, [(i, i ^ bit) for i in range(count)])  28.6 us
    dot_general x15, matrix products, dot(): lax.dot_general(a, b, (((ca,), (cb,)), ((), ())), preferred_element_type=...  25.6 us
    ppermute x4, starting transfers between devices, shared_rows(): proj_grad = proj_grad + lax.ppermute(piece, ('z', 'tp'), pairs).astype(F32)  8.54 us
    ppermute x2, starting transfers between devices, from_behind(): return lax.ppermute(array, SP, pairs)  7.7 us
    dynamic_update_slice x7, local copies, waits for them, and re-layouts, join(): out = lax.dynamic_update_slice_in_dim(out, piece, (l ^ bit) * cols, 1)  3.36 us
  transfers between devices with their start and end apart: 34, of which 15 were waited for; matrix products, arithmetic and copies ran while one was open for 18% of the time, Pallas kernels for 0%

profile of v1, /device:TPU:5, one launch (start us, length us, event | category | flops | bytes accessed | tf_op | source)
XLA Modules:
  0.0 154.9 jit_solution(6735195957790859009)
XLA Ops:
  6.2 1.4 collective-permute-start
  7.5 2.3 %collective-permute-start.1 = (bf16[112,512]{1,0:T(8,128)(2,1)S(1)}, bf16[112,512]{1,0:T(8,128)(2,1)S(1)}, u32[]{:S(2)}, u32[]{:S(2)}) collective-permute-start(bf16[112,512]{1,0:T(8,128)(2,1)S(1)} %get-tuple-element.25), channel_id=1, source_target_pairs={{0,16},{8,24},{16,0},{24,8},{1,17},{9,25},{17,1},{25,9},{2,18},{10... | collective-permute-start | bytes 344072 | tf_op jit(solution)/shard_map/ppermute | solution.py:23
  10.3 2.0 %collective-permute-done.1 = bf16[112,512]{1,0:T(8,128)(2,1)S(1)} collective-permute-done((bf16[112,512]{1,0:T(8,128)(2,1)S(1)}, bf16[112,512]{1,0:T(8,128)(2,1)S(1)}, u32[]{:S(2)}, u32[]{:S(2)}) %collective-permute-start.1) | collective-permute-done | bytes 114720 | tf_op jit(solution)/shard_map/ppermute | solution.py:23
  12.2 5.0 %collective-permute-done.2 = bf16[112,512]{1,0:T(8,128)(2,1)S(1)} collective-permute-done((bf16[112,512]{1,0:T(8,128)(2,1)S(1)}, bf16[112,512]{1,0:T(8,128)(2,1)S(1)}, u32[]{:S(2)}, u32[]{:S(2)}) %collective-permute-start.2) | collective-permute-done | bytes 114720 | tf_op jit(solution)/shard_map/ppermute | solution.py:23
  25.9 2.1 %collective-permute-done.10 = bf16[192,512]{1,0:T(8,128)(2,1)} collective-permute-done((bf16[192,512]{1,0:T(8,128)(2,1)}, bf16[192,512]{1,0:T(8,128)(2,1)}, u32[]{:S(2)}, u32[]{:S(2)}) %collective-permute-start.10) | collective-permute-done | bytes 196640 | tf_op jit(solution)/shard_map/ppermute | solution.py:23
  28.9 2.0 %collective-permute-start.11 = (bf16[96,512]{1,0:T(8,128)(2,1)S(1)}, bf16[96,512]{1,0:T(8,128)(2,1)S(1)}, u32[]{:S(2)}, u32[]{:S(2)}) collective-permute-start(bf16[96,512]{1,0:T(8,128)(2,1)S(1)} %slice.172), channel_id=1, source_target_pairs={{0,1},{1,0},{2,3},{3,2},{4,5},{5,4},{6,7},{7,6},{8,9},{9,8},{10,11... | collective-permute-start | bytes 294920 | tf_op jit(solution)/shard_map/ppermute | solution.py:23
  32.9 1.6 %constant_dynamic-update-slice_fusion.4 = bf16[192,2048]{1,0:T(8,128)(2,1)} fusion(bf16[192,2048]{1,0:T(8,128)(2,1)} %constant_dynamic-update-slice_fusion.5, bf16[192,512]{1,0:T(8,128)(2,1)} %collective-permute-done.10, s32[]{:T(128)S(6)} %select_n.104), kind=kLoop, calls=%fused_computation.111 | loop fusion | bytes 393220 | tf_op jit(solution)/shard_map/dynamic_update_slice | solution.py:98
  35.3 4.5 %collective-permute-start.13 = (bf16[192,2048]{1,0:T(8,128)(2,1)}, bf16[192,2048]{1,0:T(8,128)(2,1)S(1)}, u32[]{:S(2)}, u32[]{:S(2)}) collective-permute-start(bf16[192,2048]{1,0:T(8,128)(2,1)} %maximum_dynamic-update-slice_fusion.1), channel_id=1, source_target_pairs={{0,4},{4,0},{1,5},{5,1},{2,6},{6,2},{3,7},{7,3},{8,12},{12,8},{9,1... | collective-permute-start | bytes 2359304 | tf_op jit(solution)/shard_map/ppermute | solution.py:23
  40.1 1.3 collective-permute-start.7
  41.5 2.7 %collective-permute-done.6 = bf16[96,512]{1,0:T(8,128)(2,1)S(1)} collective-permute-done((bf16[96,512]{1,0:T(8,128)(2,1)S(1)}, bf16[96,512]{1,0:T(8,128)(2,1)S(1)}, u32[]{:S(2)}, u32[]{:S(2)}) %collective-permute-start.6) | collective-permute-done | bytes 98336 | tf_op jit(solution)/shard_map/ppermute | solution.py:23
  45.6 1.8 %collective-permute-done.3 = f32[192]{0:T(256)S(1)} collective-permute-done((f32[192]{0:T(256)S(1)}, f32[192]{0:T(256)S(1)}, u32[]{:S(2)}, u32[]{:S(2)}) %collective-permute-start.3) | collective-permute-done | bytes 800 | tf_op jit(solution)/shard_map/ppermute | solution.py:23
  47.5 2.5 %fusion.8 = f32[384,512]{1,0:T(8,128)S(1)} fusion(bf16[1,512,2048]{2,1,0:T(8,128)(2,1)S(1)} %copy-done.1, bf16[192,2048]{1,0:T(8,128)(2,1)S(1)} %collective-permute-done.13, bf16[192,2048]{1,0:T(8,128)(2,1)} %maximum_dynamic-update-slice_fusion.1), kind=kOutput, calls=%fused_computation.12 | convolution fusion | flops 808452096 | bytes 4456448 | tf_op jit(solution)/shard_map/dot_general | solution.py:27
  50.0 2.5 %fusion.5 = f32[384,512]{1,0:T(8,128)S(1)} fusion(bf16[1,512,2048]{2,1,0:T(8,128)(2,1)S(1)} %copy-done, bf16[192,2048]{1,0:T(8,128)(2,1)S(1)} %collective-permute-done.13, bf16[192,2048]{1,0:T(8,128)(2,1)} %maximum_dynamic-update-slice_fusion.1), kind=kOutput, calls=%fused_computation.9 | convolution fusion | flops 808452096 | bytes 4456448 | tf_op jit(solution)/shard_map/dot_general | solution.py:27
  56.4 1.9 %collective-permute-done.14 = bf16[192,2048]{1,0:T(8,128)(2,1)S(1)} collective-permute-done((bf16[192,2048]{1,0:T(8,128)(2,1)S(1)}, bf16[192,2048]{1,0:T(8,128)(2,1)S(1)}, u32[]{:S(2)}, u32[]{:S(2)}) %collective-permute-start.14) | collective-permute-done | bytes 786464 | tf_op jit(solution)/shard_map/ppermute | solution.py:23
  61.5 5.6 %collective-permute-start.21 = (bf16[256,2]{0,1:T(2,128)(2,1)S(1)}, bf16[256,2]{0,1:T(2,128)(2,1)S(1)}, u32[]{:S(2)}, u32[]{:S(2)}) collective-permute-start(bf16[256,2]{0,1:T(2,128)(2,1)S(1)} %slice.180), channel_id=1, source_target_pairs={{0,4},{4,8},{8,12},{12,16},{16,20},{20,24},{24,28},{1,5},{5,9},{9,... | collective-permute-start | bytes 3080 | tf_op jit(solution)/shard_map/ppermute | solution.py:18
  67.1 2.9 %collective-permute-done.17 = bf16[192,512]{1,0:T(8,128)(2,1)S(1)} collective-permute-done((bf16[192,512]{1,0:T(8,128)(2,1)S(1)}, bf16[192,512]{1,0:T(8,128)(2,1)S(1)}, u32[]{:S(2)}, u32[]{:S(2)}) %collective-permute-start.17) | collective-permute-done | bytes 196640 | tf_op jit(solution)/shard_map/ppermute | solution.py:23
  70.2 1.9 %collective-permute-start.18 = (bf16[48,512]{1,0:T(8,128)(2,1)S(1)}, bf16[48,512]{1,0:T(8,128)(2,1)S(1)}, u32[]{:S(2)}, u32[]{:S(2)}) collective-permute-start(bf16[48,512]{1,0:T(8,128)(2,1)S(1)} %get-tuple-element.32), channel_id=1, source_target_pairs={{0,8},{8,0},{16,24},{24,16},{1,9},{9,1},{17,25},{25,17},{2,10},{10... | collective-permute-start | bytes 147464 | tf_op jit(solution)/shard_map/ppermute | solution.py:23
  74.6 2.1 %collective-permute-done.19 = bf16[48,512]{1,0:T(8,128)(2,1)S(1)} collective-permute-done((bf16[48,512]{1,0:T(8,128)(2,1)S(1)}, bf16[48,512]{1,0:T(8,128)(2,1)S(1)}, u32[]{:S(2)}, u32[]{:S(2)}) %collective-permute-start.19) | collective-permute-done | bytes 49184 | tf_op jit(solution)/shard_map/ppermute | solution.py:23
  76.6 2.0 %collective-permute-done.20 = bf16[48,512]{1,0:T(8,128)(2,1)S(1)} collective-permute-done((bf16[48,512]{1,0:T(8,128)(2,1)S(1)}, bf16[48,512]{1,0:T(8,128)(2,1)S(1)}, u32[]{:S(2)}, u32[]{:S(2)}) %collective-permute-start.20) | collective-permute-done | bytes 49184 | tf_op jit(solution)/shard_map/ppermute | solution.py:23
  84.8 4.2 %collective-permute-done.32 = bf16[192,512]{1,0:T(8,128)(2,1)S(1)} collective-permute-done((bf16[192,512]{1,0:T(8,128)(2,1)S(1)}, bf16[192,512]{1,0:T(8,128)(2,1)S(1)}, u32[]{:S(2)}, u32[]{:S(2)}) %collective-permute-start.32) | collective-permute-done | bytes 196640 | tf_op jit(solution)/shard_map/ppermute | solution.py:23
  89.0 2.6 %multiply_convert_fusion.4 = (bf16[256,192]{0,1:T(8,128)(2,1)}, f32[256,192]{0,1:T(8,128)S(1)}, f32[256,192]{0,1:T(8,128)S(1)}) fusion(f32[256,194]{0,1:T(8,128)S(1)} %maximum_convert_fusion, f32[256]{0:T(256)S(1)} %bitcast.98, f32[256]{0:T(256)S(1)} %bitcast.100, f32[256]{0:T(256)S(1)} %bitcast.96, bf16[256,192]{0,1:T(8,128)(2,1)} %param.19, ...), kind=kOutput, calls=%fused_computation.77 | convolution fusion | flops 203341824 | bytes 3804160 | tf_op jit(solution)/shard_map/dot_general | solution.py:27
  91.6 1.5 collective-permute-start.22
  94.4 2.8 %fusion.2 = bf16[1,512,2048]{2,1,0:T(8,128)(2,1)} fusion(bf16[192,2048]{1,0:T(8,128)(2,1)S(1)} %copy-done.21, bf16[192,2048]{1,0:T(8,128)(2,1)S(1)} %copy-done.4, f32[384,512]{1,0:T(8,128)S(1)} %copy-done.23, f32[384,512]{1,0:T(8,128)S(1)} %copy-done.25, f32[384]{0:T(512)S(1)} %pad_maximum_fusion.8), kind=kOutput, calls=%fused_computation.6 | convolution fusion | flops 810876928 | bytes 5244416 | tf_op jit(solution)/shard_map/dot_general | solution.py:27
  97.7 1.4 fusion.18
  99.2 4.9 %collective-permute-start.25 = (bf16[4,256,256]{2,1,0:T(8,128)(2,1)S(1)}, bf16[4,256,256]{2,1,0:T(8,128)(2,1)S(1)}, u32[]{:S(2)}, u32[]{:S(2)}) collective-permute-start(bf16[4,256,256]{2,1,0:T(8,128)(2,1)S(1)} %dynamic-slice_convert_fusion), channel_id=1, source_target_pairs={{0,4},{4,0},{1,5},{5,1},{2,6},{6,2},{3,7},{7,3},{8,12},{12,8},{9,1... | collective-permute-start | bytes 1572872 | tf_op jit(solution)/shard_map/ppermute | solution.py:23
  104.2 3.7 %fusion.1 = bf16[1,512,2048]{2,1,0:T(8,128)(2,1)} fusion(bf16[384,512]{1,0:T(8,128)(2,1)S(1)} %get-tuple-element.14, bf16[192,2048]{1,0:T(8,128)(2,1)S(1)} %copy-done.19, bf16[192,2048]{1,0:T(8,128)(2,1)} %maximum_dynamic-update-slice_fusion.1), kind=kOutput, calls=%fused_computation.5 | convolution fusion | flops 809500672 | bytes 4063232 | tf_op jit(solution)/shard_map/dot_general | solution.py:27
  107.9 2.1 %collective-permute-start.33 = (f32[256,2]{0,1:T(2,128)S(1)}, f32[256,2]{0,1:T(2,128)S(1)}, u32[]{:S(2)}, u32[]{:S(2)}) collective-permute-start(f32[256,2]{0,1:T(2,128)S(1)} %slice.184), channel_id=1, source_target_pairs={{4,0},{8,4},{12,8},{16,12},{20,16},{24,20},{28,24},{5,1},{9,5},{13... | collective-permute-start | bytes 6152 | tf_op jit(solution)/shard_map/ppermute | solution.py:18
  110.0 3.7 %fusion = bf16[1,512,2048]{2,1,0:T(8,128)(2,1)} fusion(bf16[384,512]{1,0:T(8,128)(2,1)S(1)} %copy-done.12, bf16[192,2048]{1,0:T(8,128)(2,1)S(1)} %copy-done.19, bf16[192,2048]{1,0:T(8,128)(2,1)} %maximum_dynamic-update-slice_fusion.1), kind=kOutput, calls=%fused_computation.4 | convolution fusion | flops 809500672 | bytes 4063232 | tf_op jit(solution)/shard_map/dot_general | solution.py:27
  114.7 3.1 %collective-permute-start.26 = (bf16[256,256]{1,0:T(8,128)(2,1)S(1)}, bf16[256,256]{1,0:T(8,128)(2,1)S(1)}, u32[]{:S(2)}, u32[]{:S(2)}) collective-permute-start(bf16[256,256]{1,0:T(8,128)(2,1)S(1)} %get-tuple-element.19), channel_id=1, source_target_pairs={{0,0},{1,8},{2,16},{3,24},{8,1},{9,9},{10,17},{11,25},{16,2},{17,1... | collective-permute-start | bytes 393224 | tf_op jit(solution)/shard_map/ppermute | solution.py:156
  119.0 4.3 %collective-permute-start.29 = (bf16[256,256]{1,0:T(8,128)(2,1)S(1)}, bf16[256,256]{1,0:T(8,128)(2,1)S(1)}, u32[]{:S(2)}, u32[]{:S(2)}) collective-permute-start(bf16[256,256]{1,0:T(8,128)(2,1)S(1)} %get-tuple-element.20), channel_id=1, source_target_pairs={{0,3},{1,11},{2,19},{3,27},{8,2},{9,10},{10,18},{11,26},{16,1},{17... | collective-permute-start | bytes 393224 | tf_op jit(solution)/shard_map/ppermute | solution.py:156
  123.9 11.2 %collective-permute-done.26 = bf16[256,256]{1,0:T(8,128)(2,1)S(1)} collective-permute-done((bf16[256,256]{1,0:T(8,128)(2,1)S(1)}, bf16[256,256]{1,0:T(8,128)(2,1)S(1)}, u32[]{:S(2)}, u32[]{:S(2)}) %collective-permute-start.26) | collective-permute-done | bytes 131104 | tf_op jit(solution)/shard_map/ppermute | solution.py:156
  135.1 19.0 %collective-permute-done.29 = bf16[256,256]{1,0:T(8,128)(2,1)S(1)} collective-permute-done((bf16[256,256]{1,0:T(8,128)(2,1)S(1)}, bf16[256,256]{1,0:T(8,128)(2,1)S(1)}, u32[]{:S(2)}, u32[]{:S(2)}) %collective-permute-start.29) | collective-permute-done | bytes 131104 | tf_op jit(solution)/shard_map/ppermute | solution.py:156
  (170 shorter events, 40.8 us)
Async XLA Ops:
  6.2 4.1 %collective-permute-start = (bf16[112,512]{1,0:T(8,128)(2,1)S(1)}, bf16[112,512]{1,0:T(8,128)(2,1)S(1)}, u32[]{:S(2)}, u32[]{:S(2)}) collective-permute-start(bf16[112,512]{1,0:T(8,128)(2,1)S(1)} %get-tuple-element.26), channel_id=1, source_target_pairs={{0,8},{8,0},{16,24},{24,16},{1,9},{9,1},{17,25},{25,17},{2,10},{10... | collective-permute-start | bytes 344072 | tf_op jit(solution)/shard_map/ppermute | solution.py:23
  7.5 4.7 %collective-permute-start.1 = (bf16[112,512]{1,0:T(8,128)(2,1)S(1)}, bf16[112,512]{1,0:T(8,128)(2,1)S(1)}, u32[]{:S(2)}, u32[]{:S(2)}) collective-permute-start(bf16[112,512]{1,0:T(8,128)(2,1)S(1)} %get-tuple-element.25), channel_id=1, source_target_pairs={{0,16},{8,24},{16,0},{24,8},{1,17},{9,25},{17,1},{25,9},{2,18},{10... | collective-permute-start | bytes 344072 | tf_op jit(solution)/shard_map/ppermute | solution.py:23
  9.8 7.4 %collective-permute-start.2 = (bf16[112,512]{1,0:T(8,128)(2,1)S(1)}, bf16[112,512]{1,0:T(8,128)(2,1)S(1)}, u32[]{:S(2)}, u32[]{:S(2)}) collective-permute-start(bf16[112,512]{1,0:T(8,128)(2,1)S(1)} %get-tuple-element.24), channel_id=1, source_target_pairs={{0,24},{8,16},{16,8},{24,0},{1,25},{9,17},{17,9},{25,1},{2,26},{10... | collective-permute-start | bytes 344072 | tf_op jit(solution)/shard_map/ppermute | solution.py:23
  18.7 21.4 %collective-permute-start.4 = (bf16[192,512]{1,0:T(8,128)(2,1)}, bf16[192,512]{1,0:T(8,128)(2,1)S(1)}, u32[]{:S(2)}, u32[]{:S(2)}) collective-permute-start(bf16[192,512]{1,0:T(8,128)(2,1)} %get-tuple-element.33), channel_id=1, source_target_pairs={{0,1},{1,0},{2,3},{3,2},{4,5},{5,4},{6,7},{7,6},{8,9},{9,8},{10,11... | collective-permute-start | bytes 589832 | tf_op jit(solution)/shard_map/ppermute | solution.py:23
  19.9 19.9 %collective-permute-start.5 = (bf16[192,512]{1,0:T(8,128)(2,1)}, bf16[192,512]{1,0:T(8,128)(2,1)S(1)}, u32[]{:S(2)}, u32[]{:S(2)}) collective-permute-start(bf16[192,512]{1,0:T(8,128)(2,1)} %get-tuple-element.33), channel_id=1, source_target_pairs={{0,2},{1,3},{2,0},{3,1},{4,6},{5,7},{6,4},{7,5},{8,10},{9,11},{10,... | collective-permute-start | bytes 589832 | tf_op jit(solution)/shard_map/ppermute | solution.py:23
  21.9 9.0 %collective-permute-start.9 = (bf16[192,512]{1,0:T(8,128)(2,1)}, bf16[192,512]{1,0:T(8,128)(2,1)S(1)}, u32[]{:S(2)}, u32[]{:S(2)}) collective-permute-start(bf16[192,512]{1,0:T(8,128)(2,1)} %get-tuple-element.35), channel_id=1, source_target_pairs={{0,1},{1,0},{2,3},{3,2},{4,5},{5,4},{6,7},{7,6},{8,9},{9,8},{10,11... | collective-permute-start | bytes 589832 | tf_op jit(solution)/shard_map/ppermute | solution.py:23
  22.1 5.8 %collective-permute-start.10 = (bf16[192,512]{1,0:T(8,128)(2,1)}, bf16[192,512]{1,0:T(8,128)(2,1)}, u32[]{:S(2)}, u32[]{:S(2)}) collective-permute-start(bf16[192,512]{1,0:T(8,128)(2,1)} %get-tuple-element.35), channel_id=1, source_target_pairs={{0,2},{1,3},{2,0},{3,1},{4,6},{5,7},{6,4},{7,5},{8,10},{9,11},{10,... | collective-permute-start | bytes 589832 | tf_op jit(solution)/shard_map/ppermute | solution.py:23
  28.9 5.7 %collective-permute-start.11 = (bf16[96,512]{1,0:T(8,128)(2,1)S(1)}, bf16[96,512]{1,0:T(8,128)(2,1)S(1)}, u32[]{:S(2)}, u32[]{:S(2)}) collective-permute-start(bf16[96,512]{1,0:T(8,128)(2,1)S(1)} %slice.172), channel_id=1, source_target_pairs={{0,1},{1,0},{2,3},{3,2},{4,5},{5,4},{6,7},{7,6},{8,9},{9,8},{10,11... | collective-permute-start | bytes 294920 | tf_op jit(solution)/shard_map/ppermute | solution.py:23
  30.9 3.7 %collective-permute-start.12 = (bf16[96,512]{1,0:T(8,128)(2,1)S(1)}, bf16[96,512]{1,0:T(8,128)(2,1)S(1)}, u32[]{:S(2)}, u32[]{:S(2)}) collective-permute-start(bf16[96,512]{1,0:T(8,128)(2,1)S(1)} %slice.173), channel_id=1, source_target_pairs={{0,2},{1,3},{2,0},{3,1},{4,6},{5,7},{6,4},{7,5},{8,10},{9,11},{10,... | collective-permute-start | bytes 294920 | tf_op jit(solution)/shard_map/ppermute | solution.py:23
  35.3 12.2 %collective-permute-start.13 = (bf16[192,2048]{1,0:T(8,128)(2,1)}, bf16[192,2048]{1,0:T(8,128)(2,1)S(1)}, u32[]{:S(2)}, u32[]{:S(2)}) collective-permute-start(bf16[192,2048]{1,0:T(8,128)(2,1)} %maximum_dynamic-update-slice_fusion.1), channel_id=1, source_target_pairs={{0,4},{4,0},{1,5},{5,1},{2,6},{6,2},{3,7},{7,3},{8,12},{12,8},{9,1... | collective-permute-start | bytes 2359304 | tf_op jit(solution)/shard_map/ppermute | solution.py:23
  39.8 4.4 %collective-permute-start.6 = (bf16[96,512]{1,0:T(8,128)(2,1)S(1)}, bf16[96,512]{1,0:T(8,128)(2,1)S(1)}, u32[]{:S(2)}, u32[]{:S(2)}) collective-permute-start(bf16[96,512]{1,0:T(8,128)(2,1)S(1)} %slice.167), channel_id=1, source_target_pairs={{0,1},{1,0},{2,3},{3,2},{4,5},{5,4},{6,7},{7,6},{8,9},{9,8},{10,11... | collective-permute-start | bytes 294920 | tf_op jit(solution)/shard_map/ppermute | solution.py:23
  40.1 4.1 %collective-permute-start.7 = (bf16[96,512]{1,0:T(8,128)(2,1)S(1)}, bf16[96,512]{1,0:T(8,128)(2,1)S(1)}, u32[]{:S(2)}, u32[]{:S(2)}) collective-permute-start(bf16[96,512]{1,0:T(8,128)(2,1)S(1)} %slice.168), channel_id=1, source_target_pairs={{0,2},{1,3},{2,0},{3,1},{4,6},{5,7},{6,4},{7,5},{8,10},{9,11},{10,... | collective-permute-start | bytes 294920 | tf_op jit(solution)/shard_map/ppermute | solution.py:23
  44.3 8.2 %collective-permute-start.8 = (bf16[192,2048]{1,0:T(8,128)(2,1)S(1)}, bf16[192,2048]{1,0:T(8,128)(2,1)S(1)}, u32[]{:S(2)}, u32[]{:S(2)}) collective-permute-start(bf16[192,2048]{1,0:T(8,128)(2,1)S(1)} %maximum_dynamic-update-slice_fusion), channel_id=1, source_target_pairs={{0,4},{4,0},{1,5},{5,1},{2,6},{6,2},{3,7},{7,3},{8,12},{12,8},{9,1... | collective-permute-start | bytes 2359304 | tf_op jit(solution)/shard_map/ppermute | solution.py:23
  58.7 8.4 %collective-permute-start.15 = (bf16[192,512]{1,0:T(8,128)(2,1)S(1)}, bf16[192,512]{1,0:T(8,128)(2,1)S(1)}, u32[]{:S(2)}, u32[]{:S(2)}) collective-permute-start(bf16[192,512]{1,0:T(8,128)(2,1)S(1)} %get-tuple-element.16), channel_id=1, source_target_pairs={{0,1},{1,0},{2,3},{3,2},{4,5},{5,4},{6,7},{7,6},{8,9},{9,8},{10,11... | collective-permute-start | bytes 589832 | tf_op jit(solution)/shard_map/ppermute | solution.py:23
  60.0 7.1 %collective-permute-start.16 = (bf16[192,512]{1,0:T(8,128)(2,1)S(1)}, bf16[192,512]{1,0:T(8,128)(2,1)S(1)}, u32[]{:S(2)}, u32[]{:S(2)}) collective-permute-start(bf16[192,512]{1,0:T(8,128)(2,1)S(1)} %get-tuple-element.18), channel_id=1, source_target_pairs={{0,2},{1,3},{2,0},{3,1},{4,6},{5,7},{6,4},{7,5},{8,10},{9,11},{10,... | collective-permute-start | bytes 589832 | tf_op jit(solution)/shard_map/ppermute | solution.py:23
  61.2 8.9 %collective-permute-start.17 = (bf16[192,512]{1,0:T(8,128)(2,1)S(1)}, bf16[192,512]{1,0:T(8,128)(2,1)S(1)}, u32[]{:S(2)}, u32[]{:S(2)}) collective-permute-start(bf16[192,512]{1,0:T(8,128)(2,1)S(1)} %get-tuple-element.17), channel_id=1, source_target_pairs={{0,3},{1,2},{2,1},{3,0},{4,7},{5,6},{6,5},{7,4},{8,11},{9,10},{10,... | collective-permute-start | bytes 589832 | tf_op jit(solution)/shard_map/ppermute | solution.py:23
  61.5 19.1 %collective-permute-start.21 = (bf16[256,2]{0,1:T(2,128)(2,1)S(1)}, bf16[256,2]{0,1:T(2,128)(2,1)S(1)}, u32[]{:S(2)}, u32[]{:S(2)}) collective-permute-start(bf16[256,2]{0,1:T(2,128)(2,1)S(1)} %slice.180), channel_id=1, source_target_pairs={{0,4},{4,8},{8,12},{12,16},{16,20},{20,24},{24,28},{1,5},{5,9},{9,... | collective-permute-start | bytes 3080 | tf_op jit(solution)/shard_map/ppermute | solution.py:18
  70.2 4.3 %collective-permute-start.18 = (bf16[48,512]{1,0:T(8,128)(2,1)S(1)}, bf16[48,512]{1,0:T(8,128)(2,1)S(1)}, u32[]{:S(2)}, u32[]{:S(2)}) collective-permute-start(bf16[48,512]{1,0:T(8,128)(2,1)S(1)} %get-tuple-element.32), channel_id=1, source_target_pairs={{0,8},{8,0},{16,24},{24,16},{1,9},{9,1},{17,25},{25,17},{2,10},{10... | collective-permute-start | bytes 147464 | tf_op jit(solution)/shard_map/ppermute | solution.py:23
  72.2 4.4 %collective-permute-start.19 = (bf16[48,512]{1,0:T(8,128)(2,1)S(1)}, bf16[48,512]{1,0:T(8,128)(2,1)S(1)}, u32[]{:S(2)}, u32[]{:S(2)}) collective-permute-start(bf16[48,512]{1,0:T(8,128)(2,1)S(1)} %get-tuple-element.31), channel_id=1, source_target_pairs={{0,16},{8,24},{16,0},{24,8},{1,17},{9,25},{17,1},{25,9},{2,18},{10... | collective-permute-start | bytes 147464 | tf_op jit(solution)/shard_map/ppermute | solution.py:23
  73.3 5.4 %collective-permute-start.20 = (bf16[48,512]{1,0:T(8,128)(2,1)S(1)}, bf16[48,512]{1,0:T(8,128)(2,1)S(1)}, u32[]{:S(2)}, u32[]{:S(2)}) collective-permute-start(bf16[48,512]{1,0:T(8,128)(2,1)S(1)} %get-tuple-element.30), channel_id=1, source_target_pairs={{0,24},{8,16},{16,8},{24,0},{1,25},{9,17},{17,9},{25,1},{2,26},{10... | collective-permute-start | bytes 147464 | tf_op jit(solution)/shard_map/ppermute | solution.py:23
  79.0 4.7 %collective-permute-start.30 = (bf16[192,512]{1,0:T(8,128)(2,1)S(1)}, bf16[192,512]{1,0:T(8,128)(2,1)}, u32[]{:S(2)}, u32[]{:S(2)}) collective-permute-start(bf16[192,512]{1,0:T(8,128)(2,1)S(1)} %get-tuple-element.49), channel_id=1, source_target_pairs={{0,1},{1,0},{2,3},{3,2},{4,5},{5,4},{6,7},{7,6},{8,9},{9,8},{10,11... | collective-permute-start | bytes 589832 | tf_op jit(solution)/shard_map/ppermute | solution.py:23
  79.7 4.9 %collective-permute-start.31 = (bf16[192,512]{1,0:T(8,128)(2,1)S(1)}, bf16[192,512]{1,0:T(8,128)(2,1)S(1)}, u32[]{:S(2)}, u32[]{:S(2)}) collective-permute-start(bf16[192,512]{1,0:T(8,128)(2,1)S(1)} %get-tuple-element.49), channel_id=1, source_target_pairs={{0,2},{1,3},{2,0},{3,1},{4,6},{5,7},{6,4},{7,5},{8,10},{9,11},{10,... | collective-permute-start | bytes 589832 | tf_op jit(solution)/shard_map/ppermute | solution.py:23
  81.5 7.5 %collective-permute-start.32 = (bf16[192,512]{1,0:T(8,128)(2,1)S(1)}, bf16[192,512]{1,0:T(8,128)(2,1)S(1)}, u32[]{:S(2)}, u32[]{:S(2)}) collective-permute-start(bf16[192,512]{1,0:T(8,128)(2,1)S(1)} %get-tuple-element.49), channel_id=1, source_target_pairs={{0,3},{1,2},{2,1},{3,0},{4,7},{5,6},{6,5},{7,4},{8,11},{9,10},{10,... | collective-permute-start | bytes 589832 | tf_op jit(solution)/shard_map/ppermute | solution.py:23
  91.6 5.6 %collective-permute-start.22 = (bf16[256,192]{0,1:T(8,128)(2,1)S(1)}, bf16[256,192]{0,1:T(8,128)(2,1)S(1)}, u32[]{:S(2)}, u32[]{:S(2)}) collective-permute-start(bf16[256,192]{0,1:T(8,128)(2,1)S(1)} %fusion.32), channel_id=1, source_target_pairs={{0,1},{1,0},{2,3},{3,2},{4,5},{5,4},{6,7},{7,6},{8,9},{9,8},{10,11... | collective-permute-start | bytes 294920 | tf_op jit(solution)/shard_map/ppermute | solution.py:23
  93.2 4.5 %collective-permute-start.23 = (bf16[256,192]{0,1:T(8,128)(2,1)S(1)}, bf16[256,192]{0,1:T(8,128)(2,1)S(1)}, u32[]{:S(2)}, u32[]{:S(2)}) collective-permute-start(bf16[256,192]{0,1:T(8,128)(2,1)S(1)} %fusion.32), channel_id=1, source_target_pairs={{0,2},{1,3},{2,0},{3,1},{4,6},{5,7},{6,4},{7,5},{8,10},{9,11},{10,... | collective-permute-start | bytes 294920 | tf_op jit(solution)/shard_map/ppermute | solution.py:23
  93.2 4.5 %collective-permute-start.24 = (bf16[256,192]{0,1:T(8,128)(2,1)S(1)}, bf16[256,192]{0,1:T(8,128)(2,1)S(1)}, u32[]{:S(2)}, u32[]{:S(2)}) collective-permute-start(bf16[256,192]{0,1:T(8,128)(2,1)S(1)} %fusion.32), channel_id=1, source_target_pairs={{0,3},{1,2},{2,1},{3,0},{4,7},{5,6},{6,5},{7,4},{8,11},{9,10},{10,... | collective-permute-start | bytes 294920 | tf_op jit(solution)/shard_map/ppermute | solution.py:23
  99.2 15.3 %collective-permute-start.25 = (bf16[4,256,256]{2,1,0:T(8,128)(2,1)S(1)}, bf16[4,256,256]{2,1,0:T(8,128)(2,1)S(1)}, u32[]{:S(2)}, u32[]{:S(2)}) collective-permute-start(bf16[4,256,256]{2,1,0:T(8,128)(2,1)S(1)} %dynamic-slice_convert_fusion), channel_id=1, source_target_pairs={{0,4},{4,0},{1,5},{5,1},{2,6},{6,2},{3,7},{7,3},{8,12},{12,8},{9,1... | collective-permute-start | bytes 1572872 | tf_op jit(solution)/shard_map/ppermute | solution.py:23
  107.9 5.8 %collective-permute-start.33 = (f32[256,2]{0,1:T(2,128)S(1)}, f32[256,2]{0,1:T(2,128)S(1)}, u32[]{:S(2)}, u32[]{:S(2)}) collective-permute-start(f32[256,2]{0,1:T(2,128)S(1)} %slice.184), channel_id=1, source_target_pairs={{4,0},{8,4},{12,8},{16,12},{20,16},{24,20},{28,24},{5,1},{9,5},{13... | collective-permute-start | bytes 6152 | tf_op jit(solution)/shard_map/ppermute | solution.py:18
  114.7 20.4 %collective-permute-start.26 = (bf16[256,256]{1,0:T(8,128)(2,1)S(1)}, bf16[256,256]{1,0:T(8,128)(2,1)S(1)}, u32[]{:S(2)}, u32[]{:S(2)}) collective-permute-start(bf16[256,256]{1,0:T(8,128)(2,1)S(1)} %get-tuple-element.19), channel_id=1, source_target_pairs={{0,0},{1,8},{2,16},{3,24},{8,1},{9,9},{10,17},{11,25},{16,2},{17,1... | collective-permute-start | bytes 393224 | tf_op jit(solution)/shard_map/ppermute | solution.py:156
  117.9 17.2 %collective-permute-start.27 = (bf16[256,256]{1,0:T(8,128)(2,1)S(1)}, bf16[256,256]{1,0:T(8,128)(2,1)S(1)}, u32[]{:S(2)}, u32[]{:S(2)}) collective-permute-start(bf16[256,256]{1,0:T(8,128)(2,1)S(1)} %get-tuple-element.22), channel_id=1, source_target_pairs={{0,1},{1,9},{2,17},{3,25},{8,0},{9,8},{10,16},{11,24},{16,3},{17,1... | collective-permute-start | bytes 393224 | tf_op jit(solution)/shard_map/ppermute | solution.py:156
  118.8 16.3 %collective-permute-start.28 = (bf16[256,256]{1,0:T(8,128)(2,1)S(1)}, bf16[256,256]{1,0:T(8,128)(2,1)S(1)}, u32[]{:S(2)}, u32[]{:S(2)}) collective-permute-start(bf16[256,256]{1,0:T(8,128)(2,1)S(1)} %get-tuple-element.21), channel_id=1, source_target_pairs={{0,2},{1,10},{2,18},{3,26},{8,3},{9,11},{10,19},{11,27},{16,0},{17... | collective-permute-start | bytes 393224 | tf_op jit(solution)/shard_map/ppermute | solution.py:156
  119.0 35.2 %collective-permute-start.29 = (bf16[256,256]{1,0:T(8,128)(2,1)S(1)}, bf16[256,256]{1,0:T(8,128)(2,1)S(1)}, u32[]{:S(2)}, u32[]{:S(2)}) collective-permute-start(bf16[256,256]{1,0:T(8,128)(2,1)S(1)} %get-tuple-element.20), channel_id=1, source_target_pairs={{0,3},{1,11},{2,19},{3,27},{8,2},{9,10},{10,18},{11,26},{16,1},{17... | collective-permute-start | bytes 393224 | tf_op jit(solution)/shard_map/ppermute | solution.py:156
  (28 other events, 242.6 us)

commit v2 on v1

--- a/solution.py
+++ b/solution.py
@@ -1,6 +1,10 @@
+import functools
+
 import jax
 import jax.numpy as jnp
 from jax import lax
+from jax.experimental import pallas as pl
+from jax.experimental.pallas import tpu as pltpu
 from jax.sharding import Mesh
 from jax.sharding import PartitionSpec as P
 
@@ -10,6 +14,7 @@
 BF = jnp.bfloat16
 F32 = jnp.float32
 SP = ("z", "c")
+EXTRA = 16
 
 
 def from_behind(array, by):
@@ -29,6 +34,117 @@
 
 def shared_plan(sp, tp, top_routes):
     return top_routes == CORES and GROUPS * CORES == sp and tp == GROUPS and tp & (tp - 1) == 0
+
+
+def iota(shape, axis):
+    return lax.broadcasted_iota(jnp.int32, shape, axis)
+
+
+def call(kernel, outs, flops, moved, *args):
+    return pl.pallas_call(
+        kernel,
+        out_shape=outs,
+        cost_estimate=pl.CostEstimate(flops=flops, bytes_accessed=moved, transcendentals=0),
+        compiler_params=pltpu.CompilerParams(vmem_limit_bytes=48 * 1024 * 1024),
+    )(*args)
+
+
+def shape(*dims, kind=BF):
+    return jax.ShapeDtypeStruct(dims, kind)
+
+
+def sort_kernel(planes, cap, cols, routing_ref, weight_ref, x_ref, c_ref, sent_ref, perm_ref):
+    rows = planes * cap
+    z, l = lax.axis_index("z"), lax.axis_index("tp")
+    routing = routing_ref[...]
+    lane = iota((rows, 128), 1)
+    first = CORES * jnp.bitwise_xor(lane, z)
+    group = routing[:, :1]
+    hot = (group >= first) & (group < first + CORES) & (lane < planes)
+    before = (iota((rows, rows), 0) > iota((rows, rows), 1)).astype(F32).astype(BF)
+    rank = dot(before, hot.astype(F32).astype(BF), 1, 0)
+    place = jnp.sum(
+        jnp.where(hot, rank + (lane * cap).astype(F32), 0.0), axis=1, keepdims=True
+    )
+    perm = (place.astype(jnp.int32) == iota((rows, rows), 1)).astype(F32).astype(BF)
+    perm_ref[...] = perm
+    part = pl.ds(pl.multiple_of(l * cols, cols), cols)
+    x = dot(perm, x_ref[:, part], 0, 0, BF)
+    cot = dot(perm, c_ref[:, part], 0, 0, BF)
+    core = jnp.bitwise_and(routing, CORES - 1)
+    weight = weight_ref[...]
+    table = jnp.zeros((rows, 128), F32)
+    for k in range(CORES):
+        w = jnp.sum(jnp.where(core == k, weight, 0.0), axis=1, keepdims=True)
+        high = w.astype(BF).astype(F32)
+        table = jnp.where(lane == k, high, jnp.where(lane == CORES + k, w - high, table))
+    parts = dot(table.astype(BF), perm, 0, 0)[:EXTRA].astype(BF)
+    for b in range(planes):
+        sent_ref[b, :cap, :] = x[b * cap : (b + 1) * cap]
+        sent_ref[b, cap : 2 * cap, :] = cot[b * cap : (b + 1) * cap]
+        sent_ref[b, 2 * cap :, :] = jnp.zeros((EXTRA, cols), BF)
+        sent_ref[b, 2 * cap :, :rows] = parts
+
+
+def expert_kernel(planes, cap, cols, *refs):
+    pieces, (extras, wg_ref, wu_ref, wd_ref) = (refs[:5], refs[5:10]), (refs[10:12], *refs[12:15])
+    x_ref, c_ref, gg_ref, ug_ref, sh_ref, near_ref, far_ref = refs[15:22]
+    rows = planes * cap
+    c, l = lax.axis_index("c"), lax.axis_index("tp")
+    lane = iota((cap, rows), 1)
+    row = iota((cap, rows), 0)
+    scales = []
+    for side in range(2):
+        own, one, two, low, high = pieces[side]
+        for k, piece in enumerate((own, one, two, None)):
+            to = pl.ds(pl.multiple_of(jnp.bitwise_xor(l, k) * cols, cols), cols)
+            for b in range(planes):
+                part = piece[b] if piece is not None else (low[b] if b < planes // 2 else high[b - planes // 2])
+                at = pl.ds(side * rows + b * cap, cap)
+                x_ref[at, to] = part[:cap]
+                c_ref[at, to] = part[cap:]
+        for b in range(planes):
+            extra = extras[side][b].astype(F32)
+            w = extra[:CORES, :rows] + extra[CORES : 2 * CORES, :rows]
+            w = jnp.where(c == 0, w[:1], w[1:2])
+            scales.append(jnp.sum(jnp.where(lane == row + b * cap, w, 0.0), axis=1, keepdims=True))
+    scale = jnp.concatenate(scales, axis=0)
+    hid = wg_ref.shape[0]
+    step = 256
+
+    @pl.loop(0, hid // step)
+    def _(i):
+        at = pl.ds(pl.multiple_of(i * step, step), step)
+        gate = dot(x_ref[...], wg_ref[at, :], 1, 1)
+        up = dot(x_ref[...], wu_ref[at, :], 1, 1)
+        back = scale * dot(c_ref[...], wd_ref[at, :], 1, 1)
+        sig = jax.nn.sigmoid(gate)
+        act = gate * sig
+        gg_ref[:, at] = (back * up * sig * (1.0 + gate * (1.0 - sig))).astype(BF)
+        ug_ref[:, at] = (back * act).astype(BF)
+        sh_ref[:, at] = (scale * act * up).astype(BF)
+
+    lanes = wg_ref.shape[1] // cols
+
+    @pl.loop(0, lanes)
+    def _(k):
+        at = pl.ds(pl.multiple_of(jnp.bitwise_xor(l, k) * cols, cols), cols)
+        out = dot(gg_ref[...], wg_ref[:, at], 1, 0) + dot(ug_ref[...], wu_ref[:, at], 1, 0)
+        near_ref[k] = out[:rows].astype(BF)
+        far_ref[k] = out[rows:].astype(BF)
+
+
+def tail_kernel(planes, cols, own, one, two, three, cot_ref, mixer_ref, out_ref, near_ref, far_ref, act_ref, stream):
+    z, c, l = lax.axis_index("z"), lax.axis_index("c"), lax.axis_index("tp")
+    for k, piece in enumerate((own, one, two, three)):
+        at = pl.ds(pl.multiple_of(jnp.bitwise_xor(l, k) * cols, cols), cols)
+        stream[:, at] = (cot_ref[:, at].astype(F32) + piece[...].astype(F32)).astype(BF)
+    half = cols // CORES
+    for b in range(planes):
+        for ref, core in ((near_ref, c), (far_ref, 1 - c)):
+            at = (jnp.bitwise_xor(z, b) * CORES + core) * half
+            ref[b] = dot(mixer_ref[...], stream[:, pl.ds(pl.multiple_of(at, half), half)], 1, 0).astype(ref.dtype)
+    act_ref[...] = dot(out_ref[...], stream[...], 1, 1)
 
 
 def shared_rows(
@@ -37,100 +153,45 @@
 ):
     planes = lax.axis_size("z")
     lanes = lax.axis_size("tp")
-    z, c, l = lax.axis_index("z"), lax.axis_index("c"), lax.axis_index("tp")
     rows, width = moe_in.shape
     cap = rows // planes
     cols = width // lanes
-    half = cols // CORES
-    at = l * cols
-
-    group = routing[:, 0] // CORES
-    hot = (group[:, None] == jnp.arange(planes)[None, :]).astype(BF)
-    t = jnp.arange(rows)
-    before = (t[:, None] > t[None, :]).astype(BF)
-    rank = jnp.sum(dot(before, hot, 1, 0) * hot.astype(F32), axis=1).astype(jnp.int32)
-    place = group * cap + rank
-    perm = (place[:, None] == t[None, :]).astype(BF)
-
-    core = routing % CORES
-    weights = [jnp.sum(jnp.where(core == k, route_weight, 0.0), axis=1) for k in range(CORES)]
-    weights = jnp.stack(weights, axis=1)
-    high = weights.astype(BF)
-    low = (weights - high.astype(F32)).astype(BF)
-    parts = dot(jnp.concatenate([high, low], axis=1), perm, 0, 0, BF)
-    parts = parts.reshape(2 * CORES, planes, cap).transpose(1, 0, 2).reshape(planes, 1, 2 * CORES * cap)
-    parts = jnp.pad(parts, ((0, 0), (0, 15), (0, cols - 2 * CORES * cap)))
-
-    x_rows = dot(perm, lax.dynamic_slice_in_dim(moe_in, at, cols, 1), 0, 0, BF)
-    c_rows = dot(perm, lax.dynamic_slice_in_dim(cotangent, at, cols, 1), 0, 0, BF)
-    sent = jnp.concatenate(
-        [x_rows.reshape(planes, cap, cols), c_rows.reshape(planes, cap, cols), parts], axis=1
-    )
-
-    def over_planes(blocks):
-        own = lax.dynamic_index_in_dim(blocks, z, 0, False)
-        return [own] + [
-            partner(lax.dynamic_index_in_dim(blocks, z ^ bit, 0, False), "z", bit)
-            for bit in range(1, planes)
-        ]
-
-    got = over_planes(sent)
-    x_own = jnp.concatenate([g[:cap] for g in got], axis=0)
-    c_own = jnp.concatenate([g[cap : 2 * cap] for g in got], axis=0)
-    w_own = jnp.concatenate(
-        [g[2 * cap, : 2 * CORES * cap].reshape(2, CORES, cap) for g in got], axis=2
-    ).astype(F32)
-    w_own = w_own[0] + w_own[1]
-    w_mine = lax.dynamic_index_in_dim(w_own, c, 0, False)
-    w_other = lax.dynamic_index_in_dim(w_own, 1 - c, 0, False)
-    w_far = partner(w_other, "c", 1)
-    scale = jnp.concatenate([w_mine, w_far])[:, None]
-
-    def over_lanes(piece):
-        a, b = partner(piece, "tp", 1), partner(piece, "tp", 2)
-        m = piece.shape[0] // 2
-        d = jnp.concatenate([partner(b[:m], "tp", 1), partner(a[m:], "tp", 2)], axis=0)
-        return [piece, a, b, d]
-
-    def join(pieces):
-        out = jnp.zeros((pieces[0].shape[0], width), pieces[0].dtype)
-        for bit, piece in enumerate(pieces):
-            out = lax.dynamic_update_slice_in_dim(out, piece, (l ^ bit) * cols, 1)
-        return out
-
-    x_near = join(over_lanes(x_own))
-    c_near = join(over_lanes(c_own))
-    arrived = jnp.concatenate([x_near, partner(x_near, "c", 1)], axis=0)
-    arrived_cot = jnp.concatenate([c_near, partner(c_near, "c", 1)], axis=0)
-
-    gate_pre = dot(arrived, w_gate[0], 1, 1)
-    up_pre = dot(arrived, w_up[0], 1, 1)
-    sig = jax.nn.sigmoid(gate_pre)
-    hidden = gate_pre * sig * up_pre
-    hidden_grad = scale * dot(arrived_cot, w_down[0], 1, 1)
-    gate_grad = (hidden_grad * up_pre * sig * (1.0 + gate_pre * (1.0 - sig))).astype(BF)
-    up_grad = (hidden_grad * gate_pre * sig).astype(BF)
-    scaled_hidden = (scale * hidden).astype(BF)
-    partial = dot(gate_grad, w_gate[0], 1, 0) + dot(up_grad, w_up[0], 1, 0)
-    w_gate_grad = dot(gate_grad, arrived, 0, 0, BF)[None]
-    w_up_grad = dot(up_grad, arrived, 0, 0, BF)[None]
-    w_down_grad = dot(scaled_hidden, arrived_cot, 0, 0, BF)[None]
-
-    partial = partial.astype(BF)
-    near = partial[:rows].astype(F32) + partner(partial[rows:], "c", 1).astype(F32)
-    near = near.astype(BF)
-    total = lax.dynamic_slice_in_dim(near, at, cols, 1).astype(F32)
-    for bit in range(1, lanes):
-        piece = lax.dynamic_slice_in_dim(near, (l ^ bit) * cols, cols, 1)
-        total = total + partner(piece, "tp", bit).astype(F32)
+    hid = w_gate.shape[1]
+    chans = out_proj.shape[0]
+
+    sent, perm = call(
+        functools.partial(sort_kernel, planes, cap, cols),
+        (shape(planes, 2 * cap + EXTRA, cols), shape(rows, rows)),
+        4 * rows * rows * cols, 4 * rows * width * 2,
+        routing, route_weight, moe_in, cotangent,
+    )
+    got = [sent[0]] + [partner(sent[b], "z", b) for b in range(1, planes)]
+    own = jnp.stack([g[: 2 * cap] for g in got])
+    extra = jnp.stack([g[2 * cap :] for g in got])
+    one, two = partner(own, "tp", 1), partner(own, "tp", 2)
+    half = planes // 2
+    low, high = partner(two[:half], "tp", 1), partner(one[half:], "tp", 2)
+    near = [own, one, two, low, high]
+    far = [partner(piece, "c", 1) for piece in near]
+    both = 2 * rows
+    x, cot, gate_grad, up_grad, hidden, p_near, p_far = call(
+        functools.partial(expert_kernel, planes, cap, cols),
+        (shape(both, width), shape(both, width)) + (shape(both, hid),) * 3
+        + (shape(lanes, rows, cols),) * 2,
+        10 * both * hid * width, 12 * hid * width,
+        *near, *far, extra, partner(extra, "c", 1), w_gate[0], w_up[0], w_down[0],
+    )
+    w_gate_grad = dot(gate_grad, x, 0, 0, BF)[None]
+    w_up_grad = dot(up_grad, x, 0, 0, BF)[None]
+    w_down_grad = dot(hidden, cot, 0, 0, BF)[None]
+
+    p_sum = (p_near.astype(F32) + partner(p_far, "c", 1).astype(F32)).astype(BF)
+    total = p_sum[0].astype(F32)
+    for b in range(1, lanes):
+        total = total + partner(p_sum[b], "tp", b).astype(F32)
     total = total.astype(BF).reshape(planes, cap, cols)
-    back = [total[0]] + [partner(total[bit], "z", bit) for bit in range(1, planes)]
-    placed = jnp.stack(back)
-    order = z ^ jnp.arange(planes)
-    sorted_grad = jnp.zeros((planes, cap, cols), BF)
-    for bit in range(planes):
-        sorted_grad = lax.dynamic_update_index_in_dim(sorted_grad, back[bit], z ^ bit, 0)
-    moe_in_grad = dot(perm, sorted_grad.reshape(rows, cols), 1, 0, BF)
+    back = [total[0]] + [partner(total[b], "z", b) for b in range(1, planes)]
+    moe_in_grad = dot(perm, jnp.concatenate(back, axis=0), 1, 0, BF)
 
     mixed_in = (gate_c.astype(F32) * value_x.astype(F32)).astype(BF)
     earlier = from_behind(mixed_in[:, rows - (TAPS - 1) :], 1)
@@ -139,25 +200,25 @@
     for tap in range(TAPS):
         conv_out = conv_out + conv_taps[tap][:, None] * extended[:, tap : tap + rows]
     mixer_act = (gate_b.astype(F32) * conv_out).astype(BF)
-    acts = jnp.stack([mixer_act] + [partner(mixer_act, "tp", bit) for bit in range(1, lanes)])
-
-    cot_part = lax.dynamic_slice_in_dim(cotangent, at, cols, 1)
-    stream_part = (cot_part.astype(F32) + moe_in_grad.astype(F32)).astype(BF)
-    share = dot(acts.reshape(-1, rows), stream_part, 1, 0).reshape(lanes, -1, cols)
-    share_far = lax.dynamic_slice_in_dim(share, (1 - c) * half, half, 2).astype(BF)
-    share_near = lax.dynamic_slice_in_dim(share, c * half, half, 2)
-    share = (share_near + partner(share_far, "c", 1).astype(F32)).astype(BF)
-    proj_grad = jnp.zeros(share.shape[1:], F32)
-    for turn in range(lanes):
-        piece = lax.dynamic_index_in_dim(share, l ^ z ^ turn, 0, False)
-        pairs = [
-            (a * lanes + b, b * lanes + (a ^ turn)) for a in range(planes) for b in range(lanes)
-        ]
-        proj_grad = proj_grad + lax.ppermute(piece, ("z", "tp"), pairs).astype(F32)
-
-    full_grad = join([moe_in_grad] + [partner(moe_in_grad, "tp", bit) for bit in range(1, lanes)])
-    stream_grad = (cotangent.astype(F32) + full_grad.astype(F32)).astype(BF)
-    act_grad = dot(out_proj, stream_grad, 1, 1)
+
+    part = cols // CORES
+    q_near, q_far, act_grad = pl.pallas_call(
+        functools.partial(tail_kernel, planes, cols),
+        out_shape=(
+            shape(planes, chans, part, kind=F32), shape(planes, chans, part), shape(chans, rows, kind=F32),
+        ),
+        scratch_shapes=[pltpu.VMEM((rows, width), BF)],
+        cost_estimate=pl.CostEstimate(flops=4 * chans * rows * width, bytes_accessed=6 * rows * width, transcendentals=0),
+        compiler_params=pltpu.CompilerParams(vmem_limit_bytes=24 * 1024 * 1024),
+    )(
+        moe_in_grad, *[partner(moe_in_grad, "tp", b) for b in range(1, lanes)],
+        cotangent, mixer_act, out_proj,
+    )
+    q_sum = q_near + partner(q_far, "c", 1).astype(F32)
+    proj_grad = q_sum[0]
+    for b in range(1, planes):
+        proj_grad = proj_grad + partner(q_sum[b].astype(BF), "z", b).astype(F32)
+
     gate_b_grad = (act_grad * conv_out).astype(BF)
     conv_grad = act_grad * gate_b.astype(F32)
     later = from_behind(conv_grad[:, : TAPS - 1], -1)

time: 156 us -> 111 us (0.71)
  the two profiles are of different devices: /device:TPU:5 before, /device:TPU:0 now
where the time goes in v2:
time: 111 us
  waiting for transfers between devices  45 us (41%)
  starting transfers between devices  33.6 us (30%)
  Pallas kernels  11.5 us (10%)
  matrix products  8.01 us (7%)
  local copies, waits for them, and re-layouts  7.34 us (7%)
  other arithmetic  4.36 us (4%)
    ppermute x27, waiting for transfers between devices, partner(): return lax.ppermute(array, axis, [(i, i ^ bit) for i in range(count)])  44 us
    ppermute x27, starting transfers between devices, partner(): return lax.ppermute(array, axis, [(i, i ^ bit) for i in range(count)])  30.1 us
    pallas_call x2, Pallas kernels, call(): pl.pallas_call(kernel, out_shape=outs, cost_estimate=pl.CostEstimate(flop...  10.5 us
    dot_general x4, matrix products, dot(): lax.dot_general(a, b, (((ca,), (cb,)), ((), ())), preferred_element_type=...  8.01 us
    unnamed x30, local copies, waits for them, and re-layouts  6.43 us
    ppermute x2, starting transfers between devices, from_behind(): return lax.ppermute(array, SP, pairs)  3.57 us
  transfers between devices with their start and end apart: 29, of which 14 were waited for; matrix products, arithmetic and copies ran while one was open for 11% of the time, Pallas kernels for 0%

profile of v2, /device:TPU:0, one launch (start us, length us, event | category | flops | bytes accessed | tf_op | source)
XLA Modules:
  0.0 110.8 jit_solution(4319954953759614642)
XLA Ops:
  5.3 5.1 %collective-permute-start.2 = (bf16[112,512]{1,0:T(8,128)(2,1)S(1)}, bf16[112,512]{1,0:T(8,128)(2,1)S(1)}, u32[]{:S(2)}, u32[]{:S(2)}) collective-permute-start(bf16[112,512]{1,0:T(8,128)(2,1)S(1)} %get-tuple-element.53), channel_id=1, source_target_pairs={{0,24},{8,16},{16,8},{24,0},{1,25},{9,17},{17,9},{25,1},{2,26},{10... | collective-permute-start | bytes 344072 | tf_op jit(solution)/shard_map/ppermute | solution.py:28
  11.1 3.4 %collective-permute-done.2 = bf16[112,512]{1,0:T(8,128)(2,1)S(1)} collective-permute-done((bf16[112,512]{1,0:T(8,128)(2,1)S(1)}, bf16[112,512]{1,0:T(8,128)(2,1)S(1)}, u32[]{:S(2)}, u32[]{:S(2)}) %collective-permute-start.2) | collective-permute-done | bytes 114720 | tf_op jit(solution)/shard_map/ppermute | solution.py:28
  14.5 5.6 %collective-permute-done.1 = bf16[112,512]{1,0:T(8,128)(2,1)S(1)} collective-permute-done((bf16[112,512]{1,0:T(8,128)(2,1)S(1)}, bf16[112,512]{1,0:T(8,128)(2,1)S(1)}, u32[]{:S(2)}, u32[]{:S(2)}) %collective-permute-start.1) | collective-permute-done | bytes 114720 | tf_op jit(solution)/shard_map/ppermute | solution.py:28
  20.2 1.6 %collective-permute-start.4 = (bf16[4,96,512]{2,1,0:T(8,128)(2,1)S(1)}, bf16[4,96,512]{2,1,0:T(8,128)(2,1)S(1)}, u32[]{:S(2)}, u32[]{:S(2)}) collective-permute-start(bf16[4,96,512]{2,1,0:T(8,128)(2,1)S(1)} %pad_maximum_fusion.refs_0_), channel_id=1, source_target_pairs={{0,2},{1,3},{2,0},{3,1},{4,6},{5,7},{6,4},{7,5},{8,10},{9,11},{10,... | collective-permute-start | bytes 1179656 | tf_op jit(solution)/shard_map/ppermute | solution.py:28
  21.8 1.5 %collective-permute-start.3 = (bf16[4,96,512]{2,1,0:T(8,128)(2,1)S(1)}, bf16[4,96,512]{2,1,0:T(8,128)(2,1)S(1)}, u32[]{:S(2)}, u32[]{:S(2)}) collective-permute-start(bf16[4,96,512]{2,1,0:T(8,128)(2,1)S(1)} %pad_maximum_fusion.refs_0_), channel_id=1, source_target_pairs={{0,1},{1,0},{2,3},{3,2},{4,5},{5,4},{6,7},{7,6},{8,9},{9,8},{10,11... | collective-permute-start | bytes 1179656 | tf_op jit(solution)/shard_map/ppermute | solution.py:28
  23.9 6.6 %collective-permute-done.4.refs_2_ = bf16[4,96,512]{2,1,0:T(8,128)(2,1)S(1)} collective-permute-done((bf16[4,96,512]{2,1,0:T(8,128)(2,1)S(1)}, bf16[4,96,512]{2,1,0:T(8,128)(2,1)S(1)}, u32[]{:S(2)}, u32[]{:S(2)}) %collective-permute-start.4) | collective-permute-done | bytes 393248 | tf_op jit(solution)/shard_map/ppermute | solution.py:28
  30.4 1.6 %collective-permute-start.5 = (bf16[2,96,512]{2,1,0:T(8,128)(2,1)S(1)}, bf16[2,96,512]{2,1,0:T(8,128)(2,1)S(1)}, u32[]{:S(2)}, u32[]{:S(2)}) collective-permute-start(bf16[2,96,512]{2,1,0:T(8,128)(2,1)S(1)} %slice.158), channel_id=1, source_target_pairs={{0,1},{1,0},{2,3},{3,2},{4,5},{5,4},{6,7},{7,6},{8,9},{9,8},{10,11... | collective-permute-start | bytes 589832 | tf_op jit(solution)/shard_map/ppermute | solution.py:28
  32.0 1.6 %collective-permute-start.6 = (bf16[2,96,512]{2,1,0:T(8,128)(2,1)S(1)}, bf16[2,96,512]{2,1,0:T(8,128)(2,1)S(1)}, u32[]{:S(2)}, u32[]{:S(2)}) collective-permute-start(bf16[2,96,512]{2,1,0:T(8,128)(2,1)S(1)} %slice.159), channel_id=1, source_target_pairs={{0,2},{1,3},{2,0},{3,1},{4,6},{5,7},{6,4},{7,5},{8,10},{9,11},{10,... | collective-permute-start | bytes 589832 | tf_op jit(solution)/shard_map/ppermute | solution.py:28
  34.1 2.1 %collective-permute-done.5.refs_3_ = bf16[2,96,512]{2,1,0:T(8,128)(2,1)S(1)} collective-permute-done((bf16[2,96,512]{2,1,0:T(8,128)(2,1)S(1)}, bf16[2,96,512]{2,1,0:T(8,128)(2,1)S(1)}, u32[]{:S(2)}, u32[]{:S(2)}) %collective-permute-start.5) | collective-permute-done | bytes 196640 | tf_op jit(solution)/shard_map/ppermute | solution.py:28
  36.2 1.6 %collective-permute-done.6.refs_4_ = bf16[2,96,512]{2,1,0:T(8,128)(2,1)S(1)} collective-permute-done((bf16[2,96,512]{2,1,0:T(8,128)(2,1)S(1)}, bf16[2,96,512]{2,1,0:T(8,128)(2,1)S(1)}, u32[]{:S(2)}, u32[]{:S(2)}) %collective-permute-start.6) | collective-permute-done | bytes 196640 | tf_op jit(solution)/shard_map/ppermute | solution.py:28
  37.8 1.4 %collective-permute-done.11.refs_9_ = bf16[2,96,512]{2,1,0:T(8,128)(2,1)S(1)} collective-permute-done((bf16[2,96,512]{2,1,0:T(8,128)(2,1)S(1)}, bf16[2,96,512]{2,1,0:T(8,128)(2,1)S(1)}, u32[]{:S(2)}, u32[]{:S(2)}) %collective-permute-start.11) | collective-permute-done | bytes 196640 | tf_op jit(solution)/shard_map/ppermute | solution.py:28
  39.3 9.8 %shard_map.180 = (bf16[384,2048]{1,0:T(8,128)(2,1)}, bf16[384,2048]{1,0:T(8,128)(2,1)}, bf16[384,512]{1,0:T(8,128)(2,1)S(1)}, bf16[384,512]{1,0:T(8,128)(2,1)S(1...) custom-call(bf16[4,96,512]{2,1,0:T(8,128)(2,1)S(1)} %pad_maximum_fusion.refs_0_,, ...), custom_call_target="tpu_custom_call" | custom-call | flops 4026531840 | bytes 12582912 | tf_op jit(solution)/shard_map/pallas_call | solution.py:44
  50.1 2.3 %collective-permute-start.23 = (bf16[256,2]{1,0:T(8,128)(2,1)}, bf16[256,2]{1,0:T(8,128)(2,1)S(1)}, u32[]{:S(2)}, u32[]{:S(2)}) collective-permute-start(bf16[256,2]{1,0:T(8,128)(2,1)} %slice.171), channel_id=1, source_target_pairs={{0,4},{4,8},{8,12},{12,16},{16,20},{20,24},{24,28},{1,5},{5,9},{9,... | collective-permute-start | bytes 3080 | tf_op jit(solution)/shard_map/ppermute | solution.py:23
  53.6 1.3 %add_convert_fusion = bf16[4,192,512]{2,1,0:T(8,128)(2,1)S(1)} fusion(bf16[4,192,512]{2,1,0:T(8,128)(2,1)} %collective-permute-done.13, bf16[4,192,512]{2,1,0:T(8,128)(2,1)S(1)} %get-tuple-element.27), kind=kLoop, calls=%fused_computation.6 | loop fusion | flops 1572864 | bytes 2359296 | tf_op jit(solution)/shard_map/convert_element_type | solution.py:188
  55.0 1.5 %collective-permute-start.14 = (bf16[192,512]{1,0:T(8,128)(2,1)S(1)}, bf16[192,512]{1,0:T(8,128)(2,1)S(1)}, u32[]{:S(2)}, u32[]{:S(2)}) collective-permute-start(bf16[192,512]{1,0:T(8,128)(2,1)S(1)} %get-tuple-element.46), channel_id=1, source_target_pairs={{0,1},{1,0},{2,3},{3,2},{4,5},{5,4},{6,7},{7,6},{8,9},{9,8},{10,11... | collective-permute-start | bytes 589832 | tf_op jit(solution)/shard_map/ppermute | solution.py:28
  57.2 1.4 %collective-permute-start.16 = (bf16[192,512]{1,0:T(8,128)(2,1)S(1)}, bf16[192,512]{1,0:T(8,128)(2,1)S(1)}, u32[]{:S(2)}, u32[]{:S(2)}) collective-permute-start(bf16[192,512]{1,0:T(8,128)(2,1)S(1)} %get-tuple-element.47), channel_id=1, source_target_pairs={{0,3},{1,2},{2,1},{3,0},{4,7},{5,6},{6,5},{7,4},{8,11},{9,10},{10,... | collective-permute-start | bytes 589832 | tf_op jit(solution)/shard_map/ppermute | solution.py:28
  58.9 4.0 %collective-permute-done.14 = bf16[192,512]{1,0:T(8,128)(2,1)S(1)} collective-permute-done((bf16[192,512]{1,0:T(8,128)(2,1)S(1)}, bf16[192,512]{1,0:T(8,128)(2,1)S(1)}, u32[]{:S(2)}, u32[]{:S(2)}) %collective-permute-start.14) | collective-permute-done | bytes 196640 | tf_op jit(solution)/shard_map/ppermute | solution.py:28
  62.9 4.9 %collective-permute-done.15 = bf16[192,512]{1,0:T(8,128)(2,1)S(1)} collective-permute-done((bf16[192,512]{1,0:T(8,128)(2,1)S(1)}, bf16[192,512]{1,0:T(8,128)(2,1)S(1)}, u32[]{:S(2)}, u32[]{:S(2)}) %collective-permute-start.15) | collective-permute-done | bytes 196640 | tf_op jit(solution)/shard_map/ppermute | solution.py:28
  68.5 2.3 %collective-permute-start.18 = (bf16[48,512]{1,0:T(8,128)(2,1)S(1)}, bf16[48,512]{1,0:T(8,128)(2,1)S(1)}, u32[]{:S(2)}, u32[]{:S(2)}) collective-permute-start(bf16[48,512]{1,0:T(8,128)(2,1)S(1)} %get-tuple-element.59), channel_id=1, source_target_pairs={{0,16},{8,24},{16,0},{24,8},{1,17},{9,25},{17,1},{25,9},{2,18},{10... | collective-permute-start | bytes 147464 | tf_op jit(solution)/shard_map/ppermute | solution.py:28
  70.8 1.5 %collective-permute-start.19 = (bf16[48,512]{1,0:T(8,128)(2,1)S(1)}, bf16[48,512]{1,0:T(8,128)(2,1)S(1)}, u32[]{:S(2)}, u32[]{:S(2)}) collective-permute-start(bf16[48,512]{1,0:T(8,128)(2,1)S(1)} %get-tuple-element.58), channel_id=1, source_target_pairs={{0,24},{8,16},{16,8},{24,0},{1,25},{9,17},{17,9},{25,1},{2,26},{10... | collective-permute-start | bytes 147464 | tf_op jit(solution)/shard_map/ppermute | solution.py:28
  72.4 2.6 %fusion.1 = bf16[1,512,2048]{2,1,0:T(8,128)(2,1)} fusion(bf16[384,512]{1,0:T(8,128)(2,1)S(1)} %get-tuple-element.23, bf16[384,2048]{1,0:T(8,128)(2,1)S(1)} %copy-done.10), kind=kOutput, calls=%fused_computation.4 | convolution fusion | flops 806354944 | bytes 4063232 | tf_op jit(solution)/shard_map/dot_general | solution.py:32
  75.0 1.8 %collective-permute-done.19 = bf16[48,512]{1,0:T(8,128)(2,1)S(1)} collective-permute-done((bf16[48,512]{1,0:T(8,128)(2,1)S(1)}, bf16[48,512]{1,0:T(8,128)(2,1)S(1)}, u32[]{:S(2)}, u32[]{:S(2)}) %collective-permute-start.19) | collective-permute-done | bytes 49184 | tf_op jit(solution)/shard_map/ppermute | solution.py:28
  77.8 1.3 %collective-permute-start.21 = (bf16[192,512]{1,0:T(8,128)(2,1)S(1)}, bf16[192,512]{1,0:T(8,128)(2,1)S(1)}, u32[]{:S(2)}, u32[]{:S(2)}) collective-permute-start(bf16[192,512]{1,0:T(8,128)(2,1)S(1)} %convolution_convert_fusion.3.own), channel_id=1, source_target_pairs={{0,2},{1,3},{2,0},{3,1},{4,6},{5,7},{6,4},{7,5},{8,10},{9,11},{10,... | collective-permute-start | bytes 589832 | tf_op jit(solution)/shard_map/ppermute | solution.py:28
  79.1 1.5 %collective-permute-start.22 = (bf16[192,512]{1,0:T(8,128)(2,1)S(1)}, bf16[192,512]{1,0:T(8,128)(2,1)S(1)}, u32[]{:S(2)}, u32[]{:S(2)}) collective-permute-start(bf16[192,512]{1,0:T(8,128)(2,1)S(1)} %convolution_convert_fusion.3.own), channel_id=1, source_target_pairs={{0,3},{1,2},{2,1},{3,0},{4,7},{5,6},{6,5},{7,4},{8,11},{9,10},{10,... | collective-permute-start | bytes 589832 | tf_op jit(solution)/shard_map/ppermute | solution.py:28
  80.6 2.6 %fusion = bf16[1,512,2048]{2,1,0:T(8,128)(2,1)} fusion(bf16[384,512]{1,0:T(8,128)(2,1)S(1)} %get-tuple-element.21, bf16[384,2048]{1,0:T(8,128)(2,1)S(1)} %copy-done.10), kind=kOutput, calls=%fused_computation.3 | convolution fusion | flops 806354944 | bytes 4063232 | tf_op jit(solution)/shard_map/dot_general | solution.py:32
  84.4 2.6 %collective-permute-done.21.two = bf16[192,512]{1,0:T(8,128)(2,1)S(1)} collective-permute-done((bf16[192,512]{1,0:T(8,128)(2,1)S(1)}, bf16[192,512]{1,0:T(8,128)(2,1)S(1)}, u32[]{:S(2)}, u32[]{:S(2)}) %collective-permute-start.21) | collective-permute-done | bytes 196640 | tf_op jit(solution)/shard_map/ppermute | solution.py:28
  88.2 1.3 %collective-permute-start.28 = (f32[256,2]{1,0:T(8,128)S(1)}, f32[256,2]{1,0:T(8,128)S(1)}, u32[]{:S(2)}, u32[]{:S(2)}) collective-permute-start(f32[256,2]{1,0:T(8,128)S(1)} %slice.179), channel_id=1, source_target_pairs={{4,0},{8,4},{12,8},{16,12},{20,16},{24,20},{28,24},{5,1},{9,5},{13... | collective-permute-start | bytes 6152 | tf_op jit(solution)/shard_map/ppermute | solution.py:23
  89.5 2.6 %fusion.2 = bf16[1,512,2048]{2,1,0:T(8,128)(2,1)} fusion(bf16[384,512]{1,0:T(8,128)(2,1)S(1)} %get-tuple-element.24, bf16[384,2048]{1,0:T(8,128)(2,1)S(1)} %copy-done.9), kind=kOutput, calls=%fused_computation.5 | convolution fusion | flops 806354944 | bytes 4063232 | tf_op jit(solution)/shard_map/dot_general | solution.py:32
  94.5 2.8 %collective-permute-start.25 = (bf16[256,256]{1,0:T(8,128)(2,1)S(1)}, bf16[256,256]{1,0:T(8,128)(2,1)S(1)}, u32[]{:S(2)}, u32[]{:S(2)}) collective-permute-start(bf16[256,256]{1,0:T(8,128)(2,1)S(1)} %get-tuple-element.49), channel_id=1, source_target_pairs={{0,8},{8,0},{16,24},{24,16},{1,9},{9,1},{17,25},{25,17},{2,10},{10... | collective-permute-start | bytes 393224 | tf_op jit(solution)/shard_map/ppermute | solution.py:28
  97.3 2.0 %collective-permute-start.26 = (bf16[256,256]{1,0:T(8,128)(2,1)S(1)}, bf16[256,256]{1,0:T(8,128)(2,1)S(1)}, u32[]{:S(2)}, u32[]{:S(2)}) collective-permute-start(bf16[256,256]{1,0:T(8,128)(2,1)S(1)} %get-tuple-element.51), channel_id=1, source_target_pairs={{0,16},{8,24},{16,0},{24,8},{1,17},{9,25},{17,1},{25,9},{2,18},{10... | collective-permute-start | bytes 393224 | tf_op jit(solution)/shard_map/ppermute | solution.py:28
  101.3 2.1 %collective-permute-done.25 = bf16[256,256]{1,0:T(8,128)(2,1)S(1)} collective-permute-done((bf16[256,256]{1,0:T(8,128)(2,1)S(1)}, bf16[256,256]{1,0:T(8,128)(2,1)S(1)}, u32[]{:S(2)}, u32[]{:S(2)}) %collective-permute-start.25) | collective-permute-done | bytes 131104 | tf_op jit(solution)/shard_map/ppermute | solution.py:28
  103.3 6.8 %collective-permute-done.26 = bf16[256,256]{1,0:T(8,128)(2,1)S(1)} collective-permute-done((bf16[256,256]{1,0:T(8,128)(2,1)S(1)}, bf16[256,256]{1,0:T(8,128)(2,1)S(1)}, u32[]{:S(2)}, u32[]{:S(2)}) %collective-permute-start.26) | collective-permute-done | bytes 131104 | tf_op jit(solution)/shard_map/ppermute | solution.py:28
  (92 shorter events, 18.9 us)
Async XLA Ops:
  5.3 9.2 %collective-permute-start.2 = (bf16[112,512]{1,0:T(8,128)(2,1)S(1)}, bf16[112,512]{1,0:T(8,128)(2,1)S(1)}, u32[]{:S(2)}, u32[]{:S(2)}) collective-permute-start(bf16[112,512]{1,0:T(8,128)(2,1)S(1)} %get-tuple-element.53), channel_id=1, source_target_pairs={{0,24},{8,16},{16,8},{24,0},{1,25},{9,17},{17,9},{25,1},{2,26},{10... | collective-permute-start | bytes 344072 | tf_op jit(solution)/shard_map/ppermute | solution.py:28
  10.4 9.7 %collective-permute-start.1 = (bf16[112,512]{1,0:T(8,128)(2,1)S(1)}, bf16[112,512]{1,0:T(8,128)(2,1)S(1)}, u32[]{:S(2)}, u32[]{:S(2)}) collective-permute-start(bf16[112,512]{1,0:T(8,128)(2,1)S(1)} %get-tuple-element.54), channel_id=1, source_target_pairs={{0,16},{8,24},{16,0},{24,8},{1,17},{9,25},{17,1},{25,9},{2,18},{10... | collective-permute-start | bytes 344072 | tf_op jit(solution)/shard_map/ppermute | solution.py:28
  10.4 9.7 %collective-permute-start = (bf16[112,512]{1,0:T(8,128)(2,1)S(1)}, bf16[112,512]{1,0:T(8,128)(2,1)S(1)}, u32[]{:S(2)}, u32[]{:S(2)}) collective-permute-start(bf16[112,512]{1,0:T(8,128)(2,1)S(1)} %get-tuple-element.52), channel_id=1, source_target_pairs={{0,8},{8,0},{16,24},{24,16},{1,9},{9,1},{17,25},{25,17},{2,10},{10... | collective-permute-start | bytes 344072 | tf_op jit(solution)/shard_map/ppermute | solution.py:28
  20.2 10.3 %collective-permute-start.4 = (bf16[4,96,512]{2,1,0:T(8,128)(2,1)S(1)}, bf16[4,96,512]{2,1,0:T(8,128)(2,1)S(1)}, u32[]{:S(2)}, u32[]{:S(2)}) collective-permute-start(bf16[4,96,512]{2,1,0:T(8,128)(2,1)S(1)} %pad_maximum_fusion.refs_0_), channel_id=1, source_target_pairs={{0,2},{1,3},{2,0},{3,1},{4,6},{5,7},{6,4},{7,5},{8,10},{9,11},{10,... | collective-permute-start | bytes 1179656 | tf_op jit(solution)/shard_map/ppermute | solution.py:28
  21.8 10.2 %collective-permute-start.3 = (bf16[4,96,512]{2,1,0:T(8,128)(2,1)S(1)}, bf16[4,96,512]{2,1,0:T(8,128)(2,1)S(1)}, u32[]{:S(2)}, u32[]{:S(2)}) collective-permute-start(bf16[4,96,512]{2,1,0:T(8,128)(2,1)S(1)} %pad_maximum_fusion.refs_0_), channel_id=1, source_target_pairs={{0,1},{1,0},{2,3},{3,2},{4,5},{5,4},{6,7},{7,6},{8,9},{9,8},{10,11... | collective-permute-start | bytes 1179656 | tf_op jit(solution)/shard_map/ppermute | solution.py:28
  23.3 10.3 %collective-permute-start.12 = (bf16[4,16,512]{2,1,0:T(8,128)(2,1)S(1)}, bf16[4,16,512]{2,1,0:T(8,128)(2,1)S(1)}, u32[]{:S(2)}, u32[]{:S(2)}) collective-permute-start(bf16[4,16,512]{2,1,0:T(8,128)(2,1)S(1)} %pad_maximum_fusion.2.refs_10_), channel_id=1, source_target_pairs={{0,4},{4,0},{1,5},{5,1},{2,6},{6,2},{3,7},{7,3},{8,12},{12,8},{9,1... | collective-permute-start | bytes 196616 | tf_op jit(solution)/shard_map/ppermute | solution.py:28
  23.4 14.4 %collective-permute-start.7 = (bf16[4,96,512]{2,1,0:T(8,128)(2,1)S(1)}, bf16[4,96,512]{2,1,0:T(8,128)(2,1)S(1)}, u32[]{:S(2)}, u32[]{:S(2)}) collective-permute-start(bf16[4,96,512]{2,1,0:T(8,128)(2,1)S(1)} %pad_maximum_fusion.refs_0_), channel_id=1, source_target_pairs={{0,4},{4,0},{1,5},{5,1},{2,6},{6,2},{3,7},{7,3},{8,12},{12,8},{9,1... | collective-permute-start | bytes 1179656 | tf_op jit(solution)/shard_map/ppermute | solution.py:28
  30.4 5.7 %collective-permute-start.5 = (bf16[2,96,512]{2,1,0:T(8,128)(2,1)S(1)}, bf16[2,96,512]{2,1,0:T(8,128)(2,1)S(1)}, u32[]{:S(2)}, u32[]{:S(2)}) collective-permute-start(bf16[2,96,512]{2,1,0:T(8,128)(2,1)S(1)} %slice.158), channel_id=1, source_target_pairs={{0,1},{1,0},{2,3},{3,2},{4,5},{5,4},{6,7},{7,6},{8,9},{9,8},{10,11... | collective-permute-start | bytes 589832 | tf_op jit(solution)/shard_map/ppermute | solution.py:28
  32.0 5.7 %collective-permute-start.6 = (bf16[2,96,512]{2,1,0:T(8,128)(2,1)S(1)}, bf16[2,96,512]{2,1,0:T(8,128)(2,1)S(1)}, u32[]{:S(2)}, u32[]{:S(2)}) collective-permute-start(bf16[2,96,512]{2,1,0:T(8,128)(2,1)S(1)} %slice.159), channel_id=1, source_target_pairs={{0,2},{1,3},{2,0},{3,1},{4,6},{5,7},{6,4},{7,5},{8,10},{9,11},{10,... | collective-permute-start | bytes 589832 | tf_op jit(solution)/shard_map/ppermute | solution.py:28
  33.6 5.6 %collective-permute-start.8 = (bf16[4,96,512]{2,1,0:T(8,128)(2,1)S(1)}, bf16[4,96,512]{2,1,0:T(8,128)(2,1)S(1)}, u32[]{:S(2)}, u32[]{:S(2)}) collective-permute-start(bf16[4,96,512]{2,1,0:T(8,128)(2,1)S(1)} %collective-permute-done.3.refs_1_), channel_id=1, source_target_pairs={{0,4},{4,0},{1,5},{5,1},{2,6},{6,2},{3,7},{7,3},{8,12},{12,8},{9,1... | collective-permute-start | bytes 1179656 | tf_op jit(solution)/shard_map/ppermute | solution.py:28
  33.6 5.6 %collective-permute-start.9 = (bf16[4,96,512]{2,1,0:T(8,128)(2,1)S(1)}, bf16[4,96,512]{2,1,0:T(8,128)(2,1)S(1)}, u32[]{:S(2)}, u32[]{:S(2)}) collective-permute-start(bf16[4,96,512]{2,1,0:T(8,128)(2,1)S(1)} %collective-permute-done.4.refs_2_), channel_id=1, source_target_pairs={{0,4},{4,0},{1,5},{5,1},{2,6},{6,2},{3,7},{7,3},{8,12},{12,8},{9,1... | collective-permute-start | bytes 1179656 | tf_op jit(solution)/shard_map/ppermute | solution.py:28
  36.2 1.6 %collective-permute-start.10 = (bf16[2,96,512]{2,1,0:T(8,128)(2,1)S(1)}, bf16[2,96,512]{2,1,0:T(8,128)(2,1)S(1)}, u32[]{:S(2)}, u32[]{:S(2)}) collective-permute-start(bf16[2,96,512]{2,1,0:T(8,128)(2,1)S(1)} %collective-permute-done.5.refs_3_), channel_id=1, source_target_pairs={{0,4},{4,0},{1,5},{5,1},{2,6},{6,2},{3,7},{7,3},{8,12},{12,8},{9,1... | collective-permute-start | bytes 589832 | tf_op jit(solution)/shard_map/ppermute | solution.py:28
  37.8 1.4 %collective-permute-start.11 = (bf16[2,96,512]{2,1,0:T(8,128)(2,1)S(1)}, bf16[2,96,512]{2,1,0:T(8,128)(2,1)S(1)}, u32[]{:S(2)}, u32[]{:S(2)}) collective-permute-start(bf16[2,96,512]{2,1,0:T(8,128)(2,1)S(1)} %collective-permute-done.6.refs_4_), channel_id=1, source_target_pairs={{0,4},{4,0},{1,5},{5,1},{2,6},{6,2},{3,7},{7,3},{8,12},{12,8},{9,1... | collective-permute-start | bytes 589832 | tf_op jit(solution)/shard_map/ppermute | solution.py:28
  39.2 13.2 %copy-start.8 = (f32[3,256]{1,0:T(4,128)S(1)}, f32[3,256]{1,0:T(4,128)}, u32[]{:S(2)}) copy-start(f32[3,256]{1,0:T(4,128)} %param.22) | copy-start | bytes 9220
  39.2 13.2 %copy-start.7 = (bf16[256,192]{0,1:T(8,128)(2,1)S(1)}, bf16[256,192]{0,1:T(8,128)(2,1)}, u32[]{:S(2)}) copy-start(bf16[256,192]{0,1:T(8,128)(2,1)} %param.19) | copy-start | bytes 294916
  49.0 4.6 %collective-permute-start.13 = (bf16[4,192,512]{2,1,0:T(8,128)(2,1)S(1)}, bf16[4,192,512]{2,1,0:T(8,128)(2,1)}, u32[]{:S(2)}, u32[]{:S(2)}) collective-permute-start(bf16[4,192,512]{2,1,0:T(8,128)(2,1)S(1)} %get-tuple-element.28), channel_id=1, source_target_pairs={{0,4},{4,0},{1,5},{5,1},{2,6},{6,2},{3,7},{7,3},{8,12},{12,8},{9,1... | collective-permute-start | bytes 2359304 | tf_op jit(solution)/shard_map/ppermute | solution.py:28
  50.1 3.4 %collective-permute-start.23 = (bf16[256,2]{1,0:T(8,128)(2,1)}, bf16[256,2]{1,0:T(8,128)(2,1)S(1)}, u32[]{:S(2)}, u32[]{:S(2)}) collective-permute-start(bf16[256,2]{1,0:T(8,128)(2,1)} %slice.171), channel_id=1, source_target_pairs={{0,4},{4,8},{8,12},{12,16},{16,20},{20,24},{24,28},{1,5},{5,9},{9,... | collective-permute-start | bytes 3080 | tf_op jit(solution)/shard_map/ppermute | solution.py:23
  55.0 17.3 %copy-start.10 = (bf16[384,2048]{1,0:T(8,128)(2,1)S(1)}, bf16[384,2048]{1,0:T(8,128)(2,1)}, u32[]{:S(2)}) copy-start(bf16[384,2048]{1,0:T(8,128)(2,1)} %get-tuple-element.22) | copy-start | bytes 4718596
  55.0 7.8 %collective-permute-start.14 = (bf16[192,512]{1,0:T(8,128)(2,1)S(1)}, bf16[192,512]{1,0:T(8,128)(2,1)S(1)}, u32[]{:S(2)}, u32[]{:S(2)}) collective-permute-start(bf16[192,512]{1,0:T(8,128)(2,1)S(1)} %get-tuple-element.46), channel_id=1, source_target_pairs={{0,1},{1,0},{2,3},{3,2},{4,5},{5,4},{6,7},{7,6},{8,9},{9,8},{10,11... | collective-permute-start | bytes 589832 | tf_op jit(solution)/shard_map/ppermute | solution.py:28
  56.5 11.3 %collective-permute-start.15 = (bf16[192,512]{1,0:T(8,128)(2,1)S(1)}, bf16[192,512]{1,0:T(8,128)(2,1)S(1)}, u32[]{:S(2)}, u32[]{:S(2)}) collective-permute-start(bf16[192,512]{1,0:T(8,128)(2,1)S(1)} %get-tuple-element.48), channel_id=1, source_target_pairs={{0,2},{1,3},{2,0},{3,1},{4,6},{5,7},{6,4},{7,5},{8,10},{9,11},{10,... | collective-permute-start | bytes 589832 | tf_op jit(solution)/shard_map/ppermute | solution.py:28
  57.2 10.6 %collective-permute-start.16 = (bf16[192,512]{1,0:T(8,128)(2,1)S(1)}, bf16[192,512]{1,0:T(8,128)(2,1)S(1)}, u32[]{:S(2)}, u32[]{:S(2)}) collective-permute-start(bf16[192,512]{1,0:T(8,128)(2,1)S(1)} %get-tuple-element.47), channel_id=1, source_target_pairs={{0,3},{1,2},{2,1},{3,0},{4,7},{5,6},{6,5},{7,4},{8,11},{9,10},{10,... | collective-permute-start | bytes 589832 | tf_op jit(solution)/shard_map/ppermute | solution.py:28
  67.9 7.1 %collective-permute-start.17 = (bf16[48,512]{1,0:T(8,128)(2,1)S(1)}, bf16[48,512]{1,0:T(8,128)(2,1)S(1)}, u32[]{:S(2)}, u32[]{:S(2)}) collective-permute-start(bf16[48,512]{1,0:T(8,128)(2,1)S(1)} %get-tuple-element.60), channel_id=1, source_target_pairs={{0,8},{8,0},{16,24},{24,16},{1,9},{9,1},{17,25},{25,17},{2,10},{10... | collective-permute-start | bytes 147464 | tf_op jit(solution)/shard_map/ppermute | solution.py:28
  68.5 6.4 %collective-permute-start.18 = (bf16[48,512]{1,0:T(8,128)(2,1)S(1)}, bf16[48,512]{1,0:T(8,128)(2,1)S(1)}, u32[]{:S(2)}, u32[]{:S(2)}) collective-permute-start(bf16[48,512]{1,0:T(8,128)(2,1)S(1)} %get-tuple-element.59), channel_id=1, source_target_pairs={{0,16},{8,24},{16,0},{24,8},{1,17},{9,25},{17,1},{25,9},{2,18},{10... | collective-permute-start | bytes 147464 | tf_op jit(solution)/shard_map/ppermute | solution.py:28
  70.8 6.0 %collective-permute-start.19 = (bf16[48,512]{1,0:T(8,128)(2,1)S(1)}, bf16[48,512]{1,0:T(8,128)(2,1)S(1)}, u32[]{:S(2)}, u32[]{:S(2)}) collective-permute-start(bf16[48,512]{1,0:T(8,128)(2,1)S(1)} %get-tuple-element.58), channel_id=1, source_target_pairs={{0,24},{8,16},{16,8},{24,0},{1,25},{9,17},{17,9},{25,1},{2,26},{10... | collective-permute-start | bytes 147464 | tf_op jit(solution)/shard_map/ppermute | solution.py:28
  77.0 7.4 %collective-permute-start.20 = (bf16[192,512]{1,0:T(8,128)(2,1)S(1)}, bf16[192,512]{1,0:T(8,128)(2,1)S(1)}, u32[]{:S(2)}, u32[]{:S(2)}) collective-permute-start(bf16[192,512]{1,0:T(8,128)(2,1)S(1)} %convolution_convert_fusion.3.own), channel_id=1, source_target_pairs={{0,1},{1,0},{2,3},{3,2},{4,5},{5,4},{6,7},{7,6},{8,9},{9,8},{10,11... | collective-permute-start | bytes 589832 | tf_op jit(solution)/shard_map/ppermute | solution.py:28
  77.8 9.2 %collective-permute-start.21 = (bf16[192,512]{1,0:T(8,128)(2,1)S(1)}, bf16[192,512]{1,0:T(8,128)(2,1)S(1)}, u32[]{:S(2)}, u32[]{:S(2)}) collective-permute-start(bf16[192,512]{1,0:T(8,128)(2,1)S(1)} %convolution_convert_fusion.3.own), channel_id=1, source_target_pairs={{0,2},{1,3},{2,0},{3,1},{4,6},{5,7},{6,4},{7,5},{8,10},{9,11},{10,... | collective-permute-start | bytes 589832 | tf_op jit(solution)/shard_map/ppermute | solution.py:28
  79.1 8.0 %collective-permute-start.22 = (bf16[192,512]{1,0:T(8,128)(2,1)S(1)}, bf16[192,512]{1,0:T(8,128)(2,1)S(1)}, u32[]{:S(2)}, u32[]{:S(2)}) collective-permute-start(bf16[192,512]{1,0:T(8,128)(2,1)S(1)} %convolution_convert_fusion.3.own), channel_id=1, source_target_pairs={{0,3},{1,2},{2,1},{3,0},{4,7},{5,6},{6,5},{7,4},{8,11},{9,10},{10,... | collective-permute-start | bytes 589832 | tf_op jit(solution)/shard_map/ppermute | solution.py:28
  88.1 5.2 %collective-permute-start.24 = (bf16[4,256,256]{2,1,0:T(8,128)(2,1)S(1)}, bf16[4,256,256]{2,1,0:T(8,128)(2,1)}, u32[]{:S(2)}, u32[]{:S(2)}) collective-permute-start(bf16[4,256,256]{2,1,0:T(8,128)(2,1)S(1)} %get-tuple-element.30), channel_id=1, source_target_pairs={{0,4},{4,0},{1,5},{5,1},{2,6},{6,2},{3,7},{7,3},{8,12},{12,8},{9,1... | collective-permute-start | bytes 1572872 | tf_op jit(solution)/shard_map/ppermute | solution.py:28
  88.2 4.7 %collective-permute-start.28 = (f32[256,2]{1,0:T(8,128)S(1)}, f32[256,2]{1,0:T(8,128)S(1)}, u32[]{:S(2)}, u32[]{:S(2)}) collective-permute-start(f32[256,2]{1,0:T(8,128)S(1)} %slice.179), channel_id=1, source_target_pairs={{4,0},{8,4},{12,8},{16,12},{20,16},{24,20},{28,24},{5,1},{9,5},{13... | collective-permute-start | bytes 6152 | tf_op jit(solution)/shard_map/ppermute | solution.py:23
  94.5 8.8 %collective-permute-start.25 = (bf16[256,256]{1,0:T(8,128)(2,1)S(1)}, bf16[256,256]{1,0:T(8,128)(2,1)S(1)}, u32[]{:S(2)}, u32[]{:S(2)}) collective-permute-start(bf16[256,256]{1,0:T(8,128)(2,1)S(1)} %get-tuple-element.49), channel_id=1, source_target_pairs={{0,8},{8,0},{16,24},{24,16},{1,9},{9,1},{17,25},{25,17},{2,10},{10... | collective-permute-start | bytes 393224 | tf_op jit(solution)/shard_map/ppermute | solution.py:28
  97.3 12.8 %collective-permute-start.26 = (bf16[256,256]{1,0:T(8,128)(2,1)S(1)}, bf16[256,256]{1,0:T(8,128)(2,1)S(1)}, u32[]{:S(2)}, u32[]{:S(2)}) collective-permute-start(bf16[256,256]{1,0:T(8,128)(2,1)S(1)} %get-tuple-element.51), channel_id=1, source_target_pairs={{0,16},{8,24},{16,0},{24,8},{1,17},{9,25},{17,1},{25,9},{2,18},{10... | collective-permute-start | bytes 393224 | tf_op jit(solution)/shard_map/ppermute | solution.py:28
  99.3 10.8 %collective-permute-start.27 = (bf16[256,256]{1,0:T(8,128)(2,1)S(1)}, bf16[256,256]{1,0:T(8,128)(2,1)S(1)}, u32[]{:S(2)}, u32[]{:S(2)}) collective-permute-start(bf16[256,256]{1,0:T(8,128)(2,1)S(1)} %get-tuple-element.50), channel_id=1, source_target_pairs={{0,24},{8,16},{16,8},{24,0},{1,25},{9,17},{17,9},{25,1},{2,26},{10... | collective-permute-start | bytes 393224 | tf_op jit(solution)/shard_map/ppermute | solution.py:28
  (8 other events, 47.6 us)
